TPU v7x, 32 devices: a whole 2x2x4 slice. The times are simulated.
32 devices in a mesh: sp: 8 (over z, x), tp: 4 (over y, core).
Axes of the slice: x: 2, y: 2, z: 4, core: 2. Of those that a mesh axis runs over, the one named last changes fastest.
Arguments:
- residual_signal: bfloat16 [1024, 2048], P('sp', 'tp'), may hold values from -90 to 90
- lifted_signal: bfloat16 [1024, 1024], P('sp', 'tp'), may hold values from -6 to 6
- discrete_timestep: float32 [64, 1024], P('tp', 'sp'), may hold values from 0.17 to 4.2
- additional_log_fading: float32 [64, 1024], P('tp', 'sp'), may hold values from -2.1 to 0
- paired_fading: float32 [2, 32, 64], replicated, may hold values from 1.953125e-05 to 0.0625
- unpaired_fading: float32 [2, 32, 32], replicated, may hold values from 1.953125e-05 to 0.0625
- paired_twist: float32 [2, 32, 64], replicated, may hold values from -3.140625 to 3.140625
- unpaired_twist: float32 [2, 32, 32], replicated, may hold values from -3.140625 to 3.140625
- paired_latent_linears: float32 [2, 2, 2, 32, 64, 16], replicated, may hold values from -1 to 1
- unpaired_latent_linears: float32 [2, 2, 2, 32, 32, 16], replicated, may hold values from -1 to 1
- skip_coefficient: float32 [1024], replicated, may hold values from -4 to 4
- closing_norm_multiplier: float32 [1024], replicated, may hold values from 0.1 to 1.9
- emitted_linear: bfloat16 [1024, 2048], replicated, may hold values from -0.1875 to 0.1875
- leading_norm_multiplier: float32 [2048], replicated, may hold values from 0.1 to 1.9
- raising_linear: bfloat16 [2048, 8192], P('sp', 'tp'), may hold values from -0.125 to 0.125
- lowering_linear: bfloat16 [8192, 2048], P('tp', 'sp'), may hold values from -0.0625 to 0.0625
Outputs:
- layer_out: bfloat16 [1024, 2048], P('sp', 'tp')
All inputs are finite; a program needn't handle non-finite values.
Results may differ from a plain program's by a relative error of at most 0.008.
Values may be sent and summed in bfloat16 or wider, within the bound.
A program may use at most 128 MiB of HBM per device.

v0:
```python
import functools

import jax
import jax.numpy as jnp
from jax import lax
from jax.experimental import pallas as pl
from jax.experimental.pallas import tpu as pltpu
from jax.sharding import PartitionSpec as P

CHAN = 16
NORM_W = 128
EPSILON = 1e-06
SUB = 8
F32, BF16 = jnp.float32, jnp.bfloat16


def sincos(a):
    k = jnp.floor(a * 0.6366197723675814 + 0.5)
    r = a - k * 1.5703125
    r = r - k * 4.8351287841796875e-4
    r = r - k * 3.138556210e-7
    z = r * r
    s = r + r * z * (-1.6666654611e-1 + z * (8.3321608736e-3 + z * -1.9515295891e-4))
    c = 1.0 - 0.5 * z + z * z * (
        4.166664568298827e-2 + z * (-1.388731625493765e-3 + z * 2.443315711809948e-5)
    )
    half = jnp.floor(k * 0.5)
    odd = (k - 2.0 * half) > 0.5
    half_odd = (half - 2.0 * jnp.floor(half * 0.5)) > 0.5
    cos_v = jnp.where(odd, -s, c)
    sin_v = jnp.where(odd, c, s)
    return jnp.where(half_odd, -cos_v, cos_v), jnp.where(half_odd, -sin_v, sin_v)


def one_minus_exp_neg(u):
    t = jnp.full_like(u, 1.0)
    for m in range(10, 1, -1):
        t = 1.0 - u * (1.0 / m) * t
    return u * t


def cmul(ar, ai, br, bi):
    return ar * br - ai * bi, ar * bi + ai * br


def mixer_body(cfg, x_ref, dt_ref, lf_ref, long_rate, short_rate, long_freq, short_freq,
               skip_ref, gain_ref, resid_ref, lead_ref, long_hbm, short_hbm, emit_hbm, up_hbm, down_hbm,
               out_ref, lin_l, lin_s, lin_sem,
               pace, surge, pre, st, blk, ends, ends_all, cin, mg, rows_in, mrg, emit, resid_in,
               mid_out, wup, wdn, nrm, hid, part, rs_in, fin, fin_in,
               copy_sem, s_ends, r_ends, s_rows, r_rows, s_res, r_res,
               s_u1, r_u1, s_d1, r_d1, s_u2, r_u2, s_d2, r_d2, s_u3, r_u3, s_d3, r_d3,
               s_nrm, r_nrm, s_rs, r_rs, s_fin, r_fin):
    nsp, ntp, n, S, W, G, PL, PS, D, c_ff, F = cfg
    M = ntp // 2
    L = n // SUB
    half = G // 2
    SL = half * PL
    sp = lax.axis_index("sp")
    tp = lax.axis_index("tp")
    q = n // ntp
    Dl = D // ntp
    MESH = pl.DeviceIdType.MESH

    emit_copy = pltpu.make_async_copy(emit_hbm, emit, copy_sem.at[0])
    lin_copies = []
    for at in range(8):
        for kind, (src, dst) in enumerate(((long_hbm, lin_l), (short_hbm, lin_s))):
            lin_copies.append(pltpu.make_async_copy(
                src.at[at // 4, at // 2 % 2, at % 2, pl.ds(tp * half, half)], dst.at[at],
                lin_sem.at[kind, at]))
    for copy in lin_copies:
        copy.start()
    emit_copy.start()
    chunk = lax.rem(sp, c_ff)
    partner = tp + 1 - 2 * lax.rem(tp, 2)

    def cols(of):
        return pl.ds(pl.multiple_of(of * F, 128), F)

    own_up = pltpu.make_async_copy(up_hbm.at[:, cols(chunk)], wup.at[tp, sp], copy_sem.at[1])
    own_down = pltpu.make_async_copy(down_hbm.at[cols(chunk), :], wdn.at[tp, sp], copy_sem.at[2])
    own_up.start()
    own_down.start()

    def spread_copy(k, up):
        to = lax.rem(sp + k, nsp)
        src = up_hbm.at[:, cols(lax.rem(to, c_ff))] if up else down_hbm.at[cols(lax.rem(to, c_ff)), :]
        return pltpu.make_async_remote_copy(
            src_ref=src, dst_ref=(wup if up else wdn).at[tp, sp],
            send_sem=(s_u1 if up else s_d1).at[k - 1], recv_sem=(r_u1 if up else r_d1).at[k - 1],
            device_id=(to, tp), device_id_type=MESH)

    def across_copy(m, k, up):
        piece = (wup if up else wdn).at[tp, lax.rem(sp - k + nsp, nsp)]
        return pltpu.make_async_remote_copy(
            src_ref=piece, dst_ref=piece,
            send_sem=(s_u2 if up else s_d2).at[m - 1, k], recv_sem=(r_u2 if up else r_d2).at[m - 1, k],
            device_id=(sp, lax.rem(tp + 2 * m, ntp)), device_id_type=MESH)

    def pair_copy(m, up):
        piece = (wup if up else wdn).at[lax.rem(tp + 2 * m, ntp)]
        return pltpu.make_async_remote_copy(
            src_ref=piece, dst_ref=piece,
            send_sem=(s_u3 if up else s_d3).at[m], recv_sem=(r_u3 if up else r_d3).at[m],
            device_id=(sp, partner), device_id_type=MESH)

    def pass_on(first, last, up):
        for k in range(first, last):
            if k == 0:
                (own_up if up else own_down).wait()
            else:
                spread_copy(k, up).wait_recv()
            for m in range(1, M):
                across_copy(m, k, up).start()

    barrier = pltpu.get_barrier_semaphore()
    for k in range(1, nsp):
        pl.semaphore_signal(barrier, inc=1, device_id=(lax.rem(sp + k, nsp), tp), device_id_type=MESH)
    for k in range(1, ntp):
        pl.semaphore_signal(barrier, inc=1, device_id=(sp, lax.rem(tp + k, ntp)), device_id_type=MESH)
    pl.semaphore_wait(barrier, nsp + ntp - 2)

    def res_copy(k):
        to = lax.rem(tp + k, ntp)
        return pltpu.make_async_remote_copy(
            src_ref=resid_ref.at[pl.ds(to * q, q), :], dst_ref=resid_in.at[k - 1],
            send_sem=s_res.at[k - 1], recv_sem=r_res.at[k - 1],
            device_id=(sp, to), device_id_type=MESH)

    for k in range(1, nsp):
        spread_copy(k, True).start()
    for k in range(1, ntp):
        res_copy(k).start()

    lane = lax.broadcasted_iota(jnp.int32, (G, S), 1)
    group = jnp.where(lane < SL, 2 * (lane // PL), 2 * ((lane - SL) // PS) + 1)
    spread = (group == lax.broadcasted_iota(jnp.int32, (G, S), 0)).astype(F32)
    r = lax.broadcasted_iota(jnp.int32, (n, n), 0)
    t = lax.broadcasted_iota(jnp.int32, (n, n), 1)
    mix = (t == (r % SUB) * L + r // SUB).astype(F32)

    def per_state(ref):
        moved = lax.dot_general(ref[...], mix, (((1,), (1,)), ((), ())),
                                precision=lax.Precision.HIGHEST, preferred_element_type=F32)
        return lax.dot_general(moved, spread, (((0,), (0,)), ((), ())),
                               precision=lax.Precision.HIGHEST, preferred_element_type=F32)

    pace[...] = per_state(dt_ref)
    surge[...] = per_state(lf_ref)

    def flat_kind(ref, e):
        many, states = ref.shape[1:]
        width = half * states
        repeat = (lax.broadcasted_iota(jnp.int32, (states, width), 1) % states
                  == lax.broadcasted_iota(jnp.int32, (states, width), 0)).astype(F32)
        wide = jnp.dot(ref[e], repeat, precision=lax.Precision.HIGHEST, preferred_element_type=F32)
        owner = tp * half + lax.broadcasted_iota(jnp.int32, (many, width), 1) // states
        mine = owner == lax.broadcasted_iota(jnp.int32, (many, width), 0)
        return jnp.sum(jnp.where(mine, wide, 0.0), axis=0, keepdims=True)

    def flat(long_ref, short_ref, e):
        return jnp.concatenate([flat_kind(long_ref, e), flat_kind(short_ref, e)], axis=1)

    def widened(ref, index, states, sign):
        rows, width = half * CHAN, half * states
        repeat = (lax.broadcasted_iota(jnp.int32, (states, width), 1) % states
                  == lax.broadcasted_iota(jnp.int32, (states, width), 0)).astype(BF16)
        wide = jnp.dot(ref[index].reshape(rows, states).astype(BF16), repeat, preferred_element_type=F32)
        own_block = (lax.broadcasted_iota(jnp.int32, (rows, width), 0) // CHAN
                     == lax.broadcasted_iota(jnp.int32, (rows, width), 1) // states)
        return jnp.where(own_block, sign * wide, 0.0).astype(BF16)

    def block_map(index, sign=1.0):
        long_part = widened(lin_l, index, PL, sign)
        short_part = widened(lin_s, index, PS, sign)
        no_long, no_short = jnp.zeros((CHAN, SL), BF16), jnp.zeros((CHAN, S - SL), BF16)
        bands = []
        for g in range(half):
            band = slice(g * CHAN, (g + 1) * CHAN)
            bands.append(jnp.concatenate([long_part[band], no_short], axis=1))
            bands.append(jnp.concatenate([no_long, short_part[band]], axis=1))
        return jnp.concatenate(bands, axis=0)

    xv = jnp.dot(mix.astype(BF16), x_ref[...], preferred_element_type=F32).astype(BF16)
    for copy in lin_copies:
        copy.wait()
    for e in range(2):
        for c in range(2):
            st[:, pl.ds((2 * e + c) * S, S)] = jnp.dot(
                xv, block_map(4 * e + c), preferred_element_type=F32)

    for e in range(2):
        rate = flat(long_rate, short_rate, e)
        freq = flat(long_freq, short_freq, e)

        def step(i, carry):
            pr, pi, sr, si = carry
            at = i if e == 0 else L - 1 - i
            rows = pl.ds(pl.multiple_of(at * SUB, SUB), SUB)
            d = pace[rows, :]
            rd = rate * d
            m = jnp.exp(surge[rows, :] - rd)
            cos_v, sin_v = sincos(freq * d)
            w = jnp.sqrt(one_minus_exp_neg(2.0 * rd))
            ar, ai = m * cos_v, m * sin_v
            pr, pi = cmul(ar, ai, pr, pi)
            sr, si = cmul(ar, ai, sr, si)
            sr = sr + w * st[rows, pl.ds(2 * e * S, S)]
            si = si + w * st[rows, pl.ds((2 * e + 1) * S, S)]
            pre[rows, pl.ds(2 * e * S, S)] = pr
            pre[rows, pl.ds((2 * e + 1) * S, S)] = pi
            st[rows, pl.ds(2 * e * S, S)] = sr
            st[rows, pl.ds((2 * e + 1) * S, S)] = si
            return pr, pi, sr, si

        zero = jnp.zeros((SUB, S), F32)
        total = lax.fori_loop(0, L, step, (zero + 1.0, zero, zero, zero))
        for c in range(4):
            blk[4 * e + c] = total[c]
        order = range(SUB) if e == 0 else range(SUB - 1, -1, -1)
        run = None
        for b in order:
            now = tuple(blk[4 * e + c, b : b + 1, :] for c in range(4))
            if run is None:
                run = now
            else:
                p = cmul(now[0], now[1], run[0], run[1])
                s = cmul(now[0], now[1], run[2], run[3])
                run = (p[0], p[1], s[0] + now[2], s[1] + now[3])
        for c in range(4):
            ends[4 * e + c : 4 * e + c + 1, :] = run[c]

    def ends_copy(k):
        return pltpu.make_async_remote_copy(
            src_ref=ends, dst_ref=ends_all.at[k - 1],
            send_sem=s_ends.at[k - 1], recv_sem=r_ends.at[k - 1],
            device_id=(lax.rem(sp + k, nsp), tp), device_id_type=MESH)

    for k in range(1, nsp):
        ends_copy(k).start()
    for k in range(1, nsp):
        spread_copy(k, False).start()

    read = jnp.concatenate(
        [block_map(2), block_map(3, -1.0), block_map(6), block_map(7, -1.0)], axis=1)

    pass_on(0, nsp // 2, True)
    for k in range(1, nsp):
        ends_copy(k).wait_recv()
    blank = jnp.zeros((1, S), F32)

    def fold(j, carry, e):
        cr, ci = carry
        k = nsp - 1 - j if e == 0 else j + 1
        reached = k <= sp if e == 0 else nsp - k <= nsp - 1 - sp
        got = ends_all[k - 1]
        nr, ni = cmul(got[4 * e : 4 * e + 1], got[4 * e + 1 : 4 * e + 2], cr, ci)
        nr = nr + got[4 * e + 2 : 4 * e + 3]
        ni = ni + got[4 * e + 3 : 4 * e + 4]
        return jnp.where(reached, nr, cr), jnp.where(reached, ni, ci)

    for e in range(2):
        cr, ci = lax.fori_loop(0, nsp - 1, functools.partial(fold, e=e), (blank, blank))
        order = range(SUB) if e == 0 else range(SUB - 1, -1, -1)
        for b in order:
            cin[2 * e, b : b + 1, :] = cr
            cin[2 * e + 1, b : b + 1, :] = ci
            now = tuple(blk[4 * e + c, b : b + 1, :] for c in range(4))
            nr, ni = cmul(now[0], now[1], cr, ci)
            cr, ci = nr + now[2], ni + now[3]

        inr, ini = cin[2 * e], cin[2 * e + 1]

        def settle(i, _):
            rows = pl.ds(pl.multiple_of(i * SUB, SUB), SUB)
            re, im = pl.ds(2 * e * S, S), pl.ds((2 * e + 1) * S, S)
            ar, ai = cmul(pre[rows, re], pre[rows, im], inr, ini)
            st[rows, re] = st[rows, re] + ar
            st[rows, im] = st[rows, im] + ai
            return 0

        lax.fori_loop(0, L, settle, 0)

    y = lax.dot_general(st[...].astype(BF16), read, (((1,), (1,)), ((), ())),
                        preferred_element_type=F32)
    own = pl.ds(pl.multiple_of(tp * W, 128), W)
    skip_row, gain_row = skip_ref[:, own], gain_ref[:, own]
    y = y + skip_row * xv.astype(F32)
    y = 0.5 * y * (1.0 + jnp.tanh(0.7978845608028654 * (y + 0.044715 * y * y * y)))
    heads = []
    for h in range(W // NORM_W):
        head = y[:, h * NORM_W : (h + 1) * NORM_W]
        scale = lax.rsqrt(jnp.mean(head * head, axis=1, keepdims=True) + EPSILON)
        heads.append(head * scale * gain_row[:, h * NORM_W : (h + 1) * NORM_W])
    merged = jnp.concatenate(heads, axis=1).astype(BF16)
    t = lax.broadcasted_iota(jnp.int32, (n, n), 0)
    r = lax.broadcasted_iota(jnp.int32, (n, n), 1)
    unmix = (r == (t % L) * SUB + t // L).astype(BF16)
    mg[...] = jnp.dot(unmix, merged, preferred_element_type=F32).astype(BF16).reshape(ntp, q, W)

    def row_copy(k):
        to = lax.rem(tp + k, ntp)
        return pltpu.make_async_remote_copy(
            src_ref=mg.at[to], dst_ref=rows_in.at[k - 1],
            send_sem=s_rows.at[k - 1], recv_sem=r_rows.at[k - 1],
            device_id=(sp, to), device_id_type=MESH)

    for k in range(1, ntp):
        row_copy(k).start()
    pass_on(nsp // 2, nsp, True)
    emit_copy.wait()
    mrg[:, pl.ds(pl.multiple_of(tp * W, 128), W)] = mg[tp]
    mid_out[:, pl.ds(pl.multiple_of(tp * Dl, 128), Dl)] = resid_ref[pl.ds(pl.multiple_of(tp * q, q), q), :].astype(F32)
    for k in range(1, ntp):
        src = lax.rem(tp - k + ntp, ntp)
        res_copy(k).wait_recv()
        mid_out[:, pl.ds(pl.multiple_of(src * Dl, 128), Dl)] = resid_in[k - 1].astype(F32)
        row_copy(k).wait_recv()
        mrg[:, pl.ds(pl.multiple_of(src * W, 128), W)] = rows_in[k - 1]
    mid = mid_out[...] + jnp.dot(mrg[...], emit[...], preferred_element_type=F32)
    mid_out[...] = mid
    scale = lax.rsqrt(jnp.mean(mid * mid, axis=1, keepdims=True) + EPSILON)
    base, q_all = sp - chunk, c_ff * q
    nrm[chunk] = (mid * scale * lead_ref[...]).astype(BF16)

    def peer(k):
        return lax.rem(chunk + k, c_ff)

    H = c_ff // 2

    def nrm_across(m):
        return pltpu.make_async_remote_copy(
            src_ref=nrm.at[chunk], dst_ref=nrm.at[chunk],
            send_sem=s_nrm.at[0, m], recv_sem=r_nrm.at[0, m],
            device_id=(base + peer(2 * m), tp), device_id_type=MESH)

    def nrm_pair(m):
        return pltpu.make_async_remote_copy(
            src_ref=nrm.at[peer(2 * m)], dst_ref=nrm.at[peer(2 * m)],
            send_sem=s_nrm.at[1, m], recv_sem=r_nrm.at[1, m],
            device_id=(base + chunk + 1 - 2 * lax.rem(chunk, 2), tp), device_id_type=MESH)

    def rs_copy(k):
        return pltpu.make_async_remote_copy(
            src_ref=part.at[peer(k)], dst_ref=rs_in.at[k - 1],
            send_sem=s_rs.at[k - 1], recv_sem=r_rs.at[k - 1],
            device_id=(base + peer(k), tp), device_id_type=MESH)

    def fin_copy(k):
        to = lax.rem(tp + k, ntp)
        return pltpu.make_async_remote_copy(
            src_ref=fin.at[to], dst_ref=fin_in.at[k - 1],
            send_sem=s_fin.at[k - 1], recv_sem=r_fin.at[k - 1],
            device_id=(sp, to), device_id_type=MESH)

    for m in range(1, H):
        nrm_across(m).start()
    nrm_pair(0).start()
    pair_copy(0, True).start()
    pass_on(0, nsp, False)
    pair_copy(0, False).start()
    for m in range(1, H):
        nrm_across(m).wait_recv()
        nrm_pair(H - m).start()
    for up in (True, False):
        for m in range(1, M):
            for k in range(nsp):
                across_copy(m, k, up).wait_recv()
            pair_copy(M - m, up).start()
        if up:
            for m in range(M):
                pair_copy(m, True).wait_recv()
            for m in range(H):
                nrm_pair(m).wait_recv()
            rows = nrm[...].reshape(q_all, D)

            def raise_step(t, _):
                upward = jnp.dot(rows, wup[t].reshape(D, F), preferred_element_type=F32)
                hid[t] = jnp.square(jnp.maximum(upward, 0.0)).astype(BF16)
                return 0

            lax.fori_loop(0, ntp, raise_step, 0)
    for m in range(M):
        pair_copy(m, False).wait_recv()
    Dc = D // nsp
    for j in range(nsp):
        total = jnp.dot(hid[0], wdn[0, j], preferred_element_type=F32)
        for t in range(1, ntp):
            total = total + jnp.dot(hid[t], wdn[t, j], preferred_element_type=F32)
        part[:, :, j * Dc : (j + 1) * Dc] = total.astype(BF16).reshape(c_ff, q, Dc)
    for k in range(1, c_ff):
        rs_copy(k).start()
    result = mid_out[...] + part[chunk].astype(F32)
    for k in range(1, c_ff):
        rs_copy(k).wait_recv()
        result = result + rs_in[k - 1].astype(F32)
    result = result.astype(BF16)
    for t in range(ntp):
        fin[t] = result[:, t * Dl : (t + 1) * Dl]
    for k in range(1, ntp):
        fin_copy(k).start()
    out_ref[pl.ds(pl.multiple_of(tp * q, q), q), :] = fin[tp]
    for k in range(1, ntp):
        fin_copy(k).wait_recv()
        src = lax.rem(tp - k + ntp, ntp)
        out_ref[pl.ds(pl.multiple_of(src * q, q), q), :] = fin_in[k - 1]
    for k in range(1, c_ff):
        rs_copy(k).wait_send()
    for m in range(H):
        if m > 0:
            nrm_across(m).wait_send()
        nrm_pair(m).wait_send()
    for k in range(1, ntp):
        fin_copy(k).wait_send()
    for up in (True, False):
        for k in range(1, nsp):
            spread_copy(k, up).wait_send()
        for m in range(1, M):
            for k in range(nsp):
                across_copy(m, k, up).wait_send()
        for m in range(M):
            pair_copy(m, up).wait_send()
    for k in range(1, nsp):
        ends_copy(k).wait_send()
    for k in range(1, ntp):
        res_copy(k).wait_send()
        row_copy(k).wait_send()


def on_device(residual, lifted, dts, fades, long_rate, short_rate, long_freq, short_freq,
              long_lin, short_lin, skip, closing, emitted, leading, raising, lowering):
    nsp, ntp = lax.axis_size("sp"), lax.axis_size("tp")
    n, W = lifted.shape
    G = dts.shape[0]
    half = G // 2
    PL, PS = long_rate.shape[2], short_rate.shape[2]
    S = half * (PL + PS)
    D = emitted.shape[1]
    Dl = residual.shape[1]
    q = n // ntp
    c_ff = min(nsp, raising.shape[1] // 128)
    F = raising.shape[1] // c_ff
    q_all, M = c_ff * q, ntp // 2
    cfg = (nsp, ntp, n, S, W, G, PL, PS, D, c_ff, F)
    vm = pl.BlockSpec(memory_space=pltpu.VMEM)
    dma = pltpu.SemaphoreType.DMA
    return pl.pallas_call(
        functools.partial(mixer_body, cfg),
        out_shape=jax.ShapeDtypeStruct((n, Dl), BF16),
        in_specs=[vm] * 11 + [pl.BlockSpec(memory_space=pl.ANY)] * 5,
        out_specs=vm,
        scratch_shapes=[
            pltpu.VMEM((8, half, CHAN, PL), F32), pltpu.VMEM((8, half, CHAN, PS), F32), dma((2, 8)),
            pltpu.VMEM((n, S), F32), pltpu.VMEM((n, S), F32),
            pltpu.VMEM((n, 4 * S), F32), pltpu.VMEM((n, 4 * S), F32),
            pltpu.VMEM((8, SUB, S), F32), pltpu.VMEM((8, S), F32), pltpu.VMEM((nsp - 1, 8, S), F32),
            pltpu.VMEM((4, SUB, S), F32),
            pltpu.VMEM((ntp, q, W), BF16), pltpu.VMEM((ntp - 1, q, W), BF16),
            pltpu.VMEM((q, ntp * W), BF16), pltpu.VMEM(emitted.shape, BF16),
            pltpu.VMEM((ntp - 1, q, Dl), BF16),
            pltpu.VMEM((q, D), F32),
            pltpu.VMEM((ntp, nsp, D // nsp, F), BF16), pltpu.VMEM((ntp, nsp, F, D // nsp), BF16),
            pltpu.VMEM((c_ff, q, D), BF16), pltpu.VMEM((ntp, q_all, F), BF16),
            pltpu.VMEM((c_ff, q, D), BF16), pltpu.VMEM((c_ff - 1, q, D), BF16),
            pltpu.VMEM((ntp, q, Dl), BF16), pltpu.VMEM((ntp - 1, q, Dl), BF16),
            dma((3,)), dma((nsp - 1,)), dma((nsp - 1,)), dma((ntp - 1,)), dma((ntp - 1,)),
            dma((ntp - 1,)), dma((ntp - 1,)),
            *[dma((nsp - 1,))] * 4, *[dma((M - 1, nsp))] * 4, *[dma((M,))] * 4,
            *[dma((2, c_ff // 2))] * 2, *[dma((c_ff - 1,))] * 2, *[dma((ntp - 1,))] * 2,
        ],
        compiler_params=pltpu.CompilerParams(collective_id=0, has_side_effects=True),
        cost_estimate=pl.CostEstimate(flops=10**9, bytes_accessed=3 * 10**7, transcendentals=10**6),
    )(lifted, dts, fades, long_rate, short_rate, long_freq, short_freq, skip[None], closing[None],
      residual, leading[None], long_lin.swapaxes(4, 5), short_lin.swapaxes(4, 5), emitted, raising, lowering)


def solution(mesh):
    both, swapped = P("sp", "tp"), P("tp", "sp")
    in_specs = (both, both, swapped, swapped) + (P(),) * 10 + (both, swapped)
    return jax.shard_map(on_device, mesh=mesh, in_specs=in_specs, out_specs=both, check_vma=False)
```

profile of v0, /device:TPU:31, one launch (start us, length us, event | category | flops | bytes accessed | tf_op | source)
XLA Modules:
  0.0 115.9 jit_solution(8036080370142358697)
XLA Ops:
  0.0 114.3 %shard_map.154 = bf16[128,512]{1,0:T(8,128)(2,1)} custom-call(bf16[128,256]{1,0:T(8,128)(2,1)} %x_ref.1, f32[16,128]{1,0:T(8,128)} %dt_ref.1, f32[16,128]{1,0:T(8,128)} %lf_ref.1, f32[2,32,64]{2,1,0:T(8,128)} %long_rate.1, f32[2,32,32]{2,1,0:T(8,128)} %short_rate.1, f32[2,32,64]{2,1,0:T(8,128)} %long_freq.1, f32[2,32,32]{2,1,0:T(8,128)} %short_freq.1, ...), custom_call_target="tpu_custom_call" | custom-call | flops 1000000000 | bytes 30000000 | tf_op jit(solution)/shard_map/pallas_call | solution.py:448
  114.3 1.6 %copy.18 = bf16[128,512]{1,0:T(8,128)(2,1)} copy(bf16[128,512]{1,0:T(8,128)(2,1)} %shard_map.154) | data formatting | bytes 262144
where the time goes:
time: 116 us
  Pallas kernels  114 us (98%)
  local copies, waits for them, and re-layouts  1.57 us (1%)
    pallas_call x1, Pallas kernels, on_device(): pl.pallas_call(functools.partial(mixer_body, cfg), out_shape=jax.ShapeDty...  114 us

commit v1 on v0

--- a/solution.py
+++ b/solution.py
@@ -428,9 +428,670 @@
         row_copy(k).wait_send()
 
 
+def mesh_split(nsp, ntp):
+    Y = ntp // 2
+    X = Y if Y > 0 and nsp % Y == 0 else 1
+    return nsp // X, X, Y
+
+
+def paired_body(cfg, x_ref, dt_ref, lf_ref, long_rate, short_rate, long_freq, short_freq,
+                skip_ref, gain_ref, resid_ref, lead_ref, long_hbm, short_hbm, emit_hbm, up_hbm, down_hbm,
+                out_ref, lin_l, lin_s, lin_sem,
+                pace, surge, pre, st, blk, ends, ends_all, cin, mg, rows_in, mrg, emit, resid_in,
+                mid_out, wup, wdn, nrm, hid, loc, a_out, a_in, b_out, b_in, c_out, c_in, fin, fin_in,
+                copy_sem, own_sem, s_ends, r_ends, s_rows, r_rows, s_res, r_res,
+                s_z, r_z, s_x, r_x, s_d, r_d, s_t, r_t, s_y, r_y,
+                s_a, r_a, s_b, r_b, s_c, r_c, s_fin, r_fin):
+    nsp, ntp, n, S, W, G, PL, PS, D, Fz = cfg
+    Z, X, Y = mesh_split(nsp, ntp)
+    L = n // SUB
+    half = G // 2
+    SL = half * PL
+    sp = lax.axis_index("sp")
+    tp = lax.axis_index("tp")
+    q = n // ntp
+    Dl = D // ntp
+    Dh = D // nsp // 2
+    Rh = D // nsp // 2
+    MESH = pl.DeviceIdType.MESH
+    z, x, y, c = sp // X, lax.rem(sp, X), tp // 2, lax.rem(tp, 2)
+    side = z // 2
+    half_in, half_out = 1 + side, 3 * side
+    far_in, far_out = 2 - side, 3 - 3 * side
+    far0 = 2 - 2 * side
+    mate = z + 1 - 2 * lax.rem(z, 2)
+    inner, outer = z == half_in, z == half_out
+    kinds = (z, mate, far_in, far_out)
+    as_seen = 2 + jnp.where(outer, 1, 0)
+
+    def dev(z_, x_, y_, c_):
+        return (z_ * X + x_, y_ * 2 + c_)
+
+    x_mate, y_mate, c_mate = dev(z, 1 - x, y, c), dev(z, x, 1 - y, c), dev(z, x, y, 1 - c)
+
+    def remote(src, dst, ssem, rsem, to):
+        return pltpu.make_async_remote_copy(src_ref=src, dst_ref=dst, send_sem=ssem, recv_sem=rsem,
+                                            device_id=to, device_id_type=MESH)
+
+    emit_copy = pltpu.make_async_copy(emit_hbm, emit, copy_sem.at[0])
+    lin_copies = []
+    for at in range(8):
+        for kind, (src, dst) in enumerate(((long_hbm, lin_l), (short_hbm, lin_s))):
+            lin_copies.append(pltpu.make_async_copy(
+                src.at[at // 4, at // 2 % 2, at % 2, pl.ds(tp * half, half)], dst.at[at],
+                lin_sem.at[kind, at]))
+
+    def bank(up):
+        return wup if up else wdn
+
+    def shard(up, h, to):
+        part = pl.ds(pl.multiple_of(to * Fz, 128), Fz)
+        if up:
+            return up_hbm.at[pl.ds(h * Rh, Rh), part]
+        return down_hbm.at[part, pl.ds(h * Dh, Dh)]
+
+    def own_copy(up, h):
+        return pltpu.make_async_copy(shard(up, h, z), bank(up).at[c, sp, h], own_sem.at[1 - up, h])
+
+    def z_copy(up, h, k):
+        to = kinds[k]
+        return remote(shard(up, h, to), bank(up).at[c, sp, h], s_z.at[1 - up, h, k],
+                      r_z.at[1 - up, h, 1 if k == 1 else as_seen], dev(to, x, y, c))
+
+    def z_wait(up, h, k):
+        piece = bank(up).at[c, kinds[k] * X + x, h]
+        remote(piece, piece, s_z.at[1 - up, h, k], r_z.at[1 - up, h, k], x_mate).wait_recv()
+
+    def x_copy(up, h, k):
+        piece = bank(up).at[c, kinds[k] * X + x, h]
+        return remote(shard(up, h, z) if k == 0 else piece, piece,
+                      s_x.at[1 - up, h, k], r_x.at[1 - up, h, k], x_mate)
+
+    def d_copy(up, h, k, other):
+        piece = bank(up).at[c, kinds[k] * X + (1 - x if other else x), h]
+        return remote(shard(up, h, z) if k == 0 and not other else piece, piece,
+                      s_d.at[1 - up, h, k, other], r_d.at[1 - up, h, k, other], c_mate)
+
+    def hop1(up, h, k):
+        z_wait(up, h, k)
+        x_copy(up, h, k).start()
+        d_copy(up, h, k, 0).start()
+
+    def hop2(up, h, k):
+        x_copy(up, h, k).wait_recv()
+        d_copy(up, h, k, 1).start()
+
+    def hop3(up, h, k):
+        d_copy(up, h, k, 0).wait_recv()
+        d_copy(up, h, k, 1).wait_recv()
+
+    def res_copy(k):
+        to = lax.rem(tp + k, ntp)
+        return remote(resid_ref.at[pl.ds(to * q, q), :], resid_in.at[k - 1], s_res.at[k - 1], r_res.at[k - 1],
+                      (sp, to))
+
+    barrier = pltpu.get_barrier_semaphore()
+    for k in range(1, nsp):
+        pl.semaphore_signal(barrier, inc=1, device_id=(lax.rem(sp + k, nsp), tp), device_id_type=MESH)
+    for k in range(1, ntp):
+        pl.semaphore_signal(barrier, inc=1, device_id=(sp, lax.rem(tp + k, ntp)), device_id_type=MESH)
+    for copy in lin_copies:
+        copy.start()
+    emit_copy.start()
+    for up in (1, 0):
+        for h in range(2):
+            own_copy(up, h).start()
+
+    lane = lax.broadcasted_iota(jnp.int32, (G, S), 1)
+    group = jnp.where(lane < SL, 2 * (lane // PL), 2 * ((lane - SL) // PS) + 1)
+    spread = (group == lax.broadcasted_iota(jnp.int32, (G, S), 0)).astype(F32)
+    r = lax.broadcasted_iota(jnp.int32, (n, n), 0)
+    t = lax.broadcasted_iota(jnp.int32, (n, n), 1)
+    mix = (t == (r % SUB) * L + r // SUB).astype(F32)
+
+    def per_state(ref):
+        moved = lax.dot_general(ref[...], mix, (((1,), (1,)), ((), ())),
+                                precision=lax.Precision.HIGHEST, preferred_element_type=F32)
+        return lax.dot_general(moved, spread, (((0,), (0,)), ((), ())),
+                               precision=lax.Precision.HIGHEST, preferred_element_type=F32)
+
+    pace[...] = per_state(dt_ref)
+    surge[...] = per_state(lf_ref)
+
+    pl.semaphore_wait(barrier, nsp + ntp - 2)
+
+    @pl.when(inner)
+    def _():
+        for k in (2, 3):
+            z_copy(1, 0, k).start()
+
+    for h in range(2):
+        z_copy(1, h, 1).start()
+        x_copy(1, h, 0).start()
+        d_copy(1, h, 0, 0).start()
+    for k in range(1, ntp):
+        res_copy(k).start()
+
+    def flat_kind(ref, e):
+        many, states = ref.shape[1:]
+        width = half * states
+        repeat = (lax.broadcasted_iota(jnp.int32, (states, width), 1) % states
+                  == lax.broadcasted_iota(jnp.int32, (states, width), 0)).astype(F32)
+        wide = jnp.dot(ref[e], repeat, precision=lax.Precision.HIGHEST, preferred_element_type=F32)
+        owner = tp * half + lax.broadcasted_iota(jnp.int32, (many, width), 1) // states
+        mine = owner == lax.broadcasted_iota(jnp.int32, (many, width), 0)
+        return jnp.sum(jnp.where(mine, wide, 0.0), axis=0, keepdims=True)
+
+    def flat(long_ref, short_ref, e):
+        return jnp.concatenate([flat_kind(long_ref, e), flat_kind(short_ref, e)], axis=1)
+
+    def widened(ref, index, states, sign):
+        rows, width = half * CHAN, half * states
+        repeat = (lax.broadcasted_iota(jnp.int32, (states, width), 1) % states
+                  == lax.broadcasted_iota(jnp.int32, (states, width), 0)).astype(BF16)
+        wide = jnp.dot(ref[index].reshape(rows, states).astype(BF16), repeat, preferred_element_type=F32)
+        own_block = (lax.broadcasted_iota(jnp.int32, (rows, width), 0) // CHAN
+                     == lax.broadcasted_iota(jnp.int32, (rows, width), 1) // states)
+        return jnp.where(own_block, sign * wide, 0.0).astype(BF16)
+
+    def block_map(index, sign=1.0):
+        long_part = widened(lin_l, index, PL, sign)
+        short_part = widened(lin_s, index, PS, sign)
+        no_long, no_short = jnp.zeros((CHAN, SL), BF16), jnp.zeros((CHAN, S - SL), BF16)
+        bands = []
+        for g in range(half):
+            band = slice(g * CHAN, (g + 1) * CHAN)
+            bands.append(jnp.concatenate([long_part[band], no_short], axis=1))
+            bands.append(jnp.concatenate([no_long, short_part[band]], axis=1))
+        return jnp.concatenate(bands, axis=0)
+
+    xv = jnp.dot(mix.astype(BF16), x_ref[...], preferred_element_type=F32).astype(BF16)
+    for copy in lin_copies:
+        copy.wait()
+    for e in range(2):
+        for part in range(2):
+            st[:, pl.ds((2 * e + part) * S, S)] = jnp.dot(
+                xv, block_map(4 * e + part), preferred_element_type=F32)
+
+    for e in range(2):
+        rate = flat(long_rate, short_rate, e)
+        freq = flat(long_freq, short_freq, e)
+
+        def step(i, carry):
+            pr, pi, sr, si = carry
+            at = i if e == 0 else L - 1 - i
+            rows = pl.ds(pl.multiple_of(at * SUB, SUB), SUB)
+            d = pace[rows, :]
+            rd = rate * d
+            m = jnp.exp(surge[rows, :] - rd)
+            cos_v, sin_v = sincos(freq * d)
+            w = jnp.sqrt(one_minus_exp_neg(2.0 * rd))
+            ar, ai = m * cos_v, m * sin_v
+            pr, pi = cmul(ar, ai, pr, pi)
+            sr, si = cmul(ar, ai, sr, si)
+            sr = sr + w * st[rows, pl.ds(2 * e * S, S)]
+            si = si + w * st[rows, pl.ds((2 * e + 1) * S, S)]
+            pre[rows, pl.ds(2 * e * S, S)] = pr
+            pre[rows, pl.ds((2 * e + 1) * S, S)] = pi
+            st[rows, pl.ds(2 * e * S, S)] = sr
+            st[rows, pl.ds((2 * e + 1) * S, S)] = si
+            return pr, pi, sr, si
+
+        zero = jnp.zeros((SUB, S), F32)
+        total = lax.fori_loop(0, L, step, (zero + 1.0, zero, zero, zero))
+        for part in range(4):
+            blk[4 * e + part] = total[part]
+        order = range(SUB) if e == 0 else range(SUB - 1, -1, -1)
+        run = None
+        for b in order:
+            now = tuple(blk[4 * e + part, b : b + 1, :] for part in range(4))
+            if run is None:
+                run = now
+            else:
+                p = cmul(now[0], now[1], run[0], run[1])
+                s = cmul(now[0], now[1], run[2], run[3])
+                run = (p[0], p[1], s[0] + now[2], s[1] + now[3])
+        for part in range(4):
+            ends[e, part : part + 1, :] = run[part]
+
+    def ends_copy(e, k):
+        return remote(ends.at[e], ends_all.at[e, k - 1], s_ends.at[e, k - 1], r_ends.at[e, k - 1],
+                      (sp + k if e == 0 else sp - k, tp))
+
+    def has_after(e, k):
+        return sp + k < nsp if e == 0 else sp >= k
+
+    def has_before(e, k):
+        return has_after(1 - e, k)
+
+    def ends_do(e, k, send, act):
+        @pl.when(has_after(e, k) if send else has_before(e, k))
+        def _():
+            act(ends_copy(e, k))
+
+    for k in range(1, nsp):
+        for e in range(2):
+            ends_do(e, k, True, lambda copy: copy.start())
+
+    @pl.when(inner)
+    def _():
+        for k in (2, 3):
+            z_copy(1, 1, k).start()
+
+    @pl.when(outer)
+    def _():
+        for k in (2, 3):
+            z_copy(1, 0, k).start()
+
+    read = jnp.concatenate(
+        [block_map(2), block_map(3, -1.0), block_map(6), block_map(7, -1.0)], axis=1)
+
+    for h in range(2):
+        hop1(1, h, 1)
+    for h in range(2):
+        hop2(1, h, 0)
+    hop1(1, 0, 2)
+
+    @pl.when(inner)
+    def _():
+        for h in range(2):
+            z_copy(0, h, 1).start()
+
+    for h in range(2):
+        x_copy(0, h, 0).start()
+        d_copy(0, h, 0, 0).start()
+    for k in range(nsp - 1, 0, -1):
+        for e in range(2):
+            ends_do(e, k, False, lambda copy: copy.wait_recv())
+    blank = jnp.zeros((1, S), F32)
+
+    def fold(j, carry, e):
+        cr, ci = carry
+        k = nsp - 1 - j
+        got = ends_all[e, k - 1]
+        nr, ni = cmul(got[0:1], got[1:2], cr, ci)
+        reached = has_before(e, k)
+        return jnp.where(reached, nr + got[2:3], cr), jnp.where(reached, ni + got[3:4], ci)
+
+    for e in range(2):
+        cr, ci = lax.fori_loop(0, nsp - 1, functools.partial(fold, e=e), (blank, blank))
+        order = range(SUB) if e == 0 else range(SUB - 1, -1, -1)
+        for b in order:
+            cin[2 * e, b : b + 1, :] = cr
+            cin[2 * e + 1, b : b + 1, :] = ci
+            now = tuple(blk[4 * e + part, b : b + 1, :] for part in range(4))
+            nr, ni = cmul(now[0], now[1], cr, ci)
+            cr, ci = nr + now[2], ni + now[3]
+
+        inr, ini = cin[2 * e], cin[2 * e + 1]
+
+        def settle(i, _):
+            rows = pl.ds(pl.multiple_of(i * SUB, SUB), SUB)
+            re, im = pl.ds(2 * e * S, S), pl.ds((2 * e + 1) * S, S)
+            ar, ai = cmul(pre[rows, re], pre[rows, im], inr, ini)
+            st[rows, re] = st[rows, re] + ar
+            st[rows, im] = st[rows, im] + ai
+            return 0
+
+        lax.fori_loop(0, L, settle, 0)
+
+    v = lax.dot_general(st[...].astype(BF16), read, (((1,), (1,)), ((), ())),
+                        preferred_element_type=F32)
+    own = pl.ds(pl.multiple_of(tp * W, 128), W)
+    skip_row, gain_row = skip_ref[:, own], gain_ref[:, own]
+    v = v + skip_row * xv.astype(F32)
+    v = 0.5 * v * (1.0 + jnp.tanh(0.7978845608028654 * (v + 0.044715 * v * v * v)))
+    heads = []
+    for h in range(W // NORM_W):
+        head = v[:, h * NORM_W : (h + 1) * NORM_W]
+        scale = lax.rsqrt(jnp.mean(head * head, axis=1, keepdims=True) + EPSILON)
+        heads.append(head * scale * gain_row[:, h * NORM_W : (h + 1) * NORM_W])
+    merged = jnp.concatenate(heads, axis=1).astype(BF16)
+    t = lax.broadcasted_iota(jnp.int32, (n, n), 0)
+    r = lax.broadcasted_iota(jnp.int32, (n, n), 1)
+    unmix = (r == (t % L) * SUB + t // L).astype(BF16)
+    mg[...] = jnp.dot(unmix, merged, preferred_element_type=F32).astype(BF16).reshape(ntp, q, W)
+
+    def row_copy(k):
+        to = lax.rem(tp + k, ntp)
+        return remote(mg.at[to], rows_in.at[k - 1], s_rows.at[k - 1], r_rows.at[k - 1], (sp, to))
+
+    for k in range(1, ntp):
+        row_copy(k).start()
+    emit_copy.wait()
+    mrg[:, pl.ds(pl.multiple_of(tp * W, 128), W)] = mg[tp]
+    mid_out[:, pl.ds(pl.multiple_of(tp * Dl, 128), Dl)] = resid_ref[pl.ds(pl.multiple_of(tp * q, q), q), :].astype(F32)
+    for k in range(1, ntp):
+        src = lax.rem(tp - k + ntp, ntp)
+        res_copy(k).wait_recv()
+        mid_out[:, pl.ds(pl.multiple_of(src * Dl, 128), Dl)] = resid_in[k - 1].astype(F32)
+        row_copy(k).wait_recv()
+        mrg[:, pl.ds(pl.multiple_of(src * W, 128), W)] = rows_in[k - 1]
+    mid = mid_out[...] + jnp.dot(mrg[...], emit[...], preferred_element_type=F32)
+    mid_out[...] = mid
+    scale = lax.rsqrt(jnp.mean(mid * mid, axis=1, keepdims=True) + EPSILON)
+    nrm[0, z] = (mid * scale * lead_ref[...]).astype(BF16)
+
+    def t_far():
+        return remote(nrm.at[0, z], nrm.at[0, z], s_t.at[0], r_t.at[as_seen], dev(far_in, x, y, c))
+
+    def t_mate(k):
+        block = nrm.at[0, kinds[k]]
+        return remote(block, block, s_t.at[max(k, 1)], r_t.at[max(k, 1)], dev(mate, x, y, c))
+
+    def t_wait(k):
+        t_mate(k).wait_recv()
+
+    def y_copy(k):
+        return remote(nrm.at[0, kinds[k]], nrm.at[1, kinds[k]], s_y.at[k], r_y.at[k], y_mate)
+
+    t_far().start()
+    t_mate(0).start()
+    y_copy(0).start()
+
+    @pl.when(outer)
+    def _():
+        for k in (2, 3):
+            z_copy(1, 1, k).start()
+        for h in range(2):
+            z_copy(0, h, 1).start()
+
+    for h in range(2):
+        hop2(1, h, 1)
+    hop2(1, 0, 2)
+    hop1(1, 1, 2)
+    hop1(1, 0, 3)
+    t_wait(1)
+    y_copy(1).start()
+
+    @pl.when(outer)
+    def _():
+        for h in range(2):
+            hop1(0, h, 1)
+
+    for h in range(2):
+        hop2(0, h, 0)
+    hop2(1, 1, 2)
+    for k in (2, 3):
+        t_wait(k)
+
+        @pl.when(inner)
+        def _():
+            t_mate(k).start()
+
+        y_copy(k).start()
+
+    @pl.when(inner)
+    def _():
+        z_copy(0, 0, 3).start()
+
+    @pl.when(outer)
+    def _():
+        for h in range(2):
+            for k in (2, 3):
+                z_copy(0, h, k).start()
+
+    hop2(1, 0, 3)
+    hop1(1, 1, 3)
+
+    @pl.when(inner)
+    def _():
+        z_copy(0, 0, 2).start()
+        for k in (2, 3):
+            z_copy(0, 1, k).start()
+
+    hop2(1, 1, 3)
+    for k in range(4):
+        y_copy(k).wait_recv()
+    for h in range(2):
+        own_copy(1, h).wait()
+        for k in range(4):
+            hop3(1, h, k)
+    rows = nrm[...].reshape(2 * Z * q, D)
+    for b in range(2):
+        upward = jnp.dot(rows, wup[b].reshape(D, Fz), preferred_element_type=F32)
+        hid[b] = jnp.square(jnp.maximum(upward, 0.0)).astype(BF16)
+
+    def cols(zs, x_, h):
+        return pl.ds(pl.multiple_of((zs * X + x_) * 2 * Dh + h * Dh, 128), Dh)
+
+    def a_copy(zs, h):
+        g = zs * 2 + h
+        return remote(a_out.at[g], a_in.at[g], s_a.at[g], r_a.at[g], y_mate)
+
+    def b_copy(zs, h):
+        g = zs * 2 + h
+        return remote(b_out.at[g, mate], b_in.at[g, mate], s_b.at[0, g], r_b.at[0, g], dev(mate, x, y, c))
+
+    def b_far(zs, h):
+        g = zs * 2 + h
+        blocks = pl.ds(far0, 2)
+        return remote(b_out.at[g, blocks], b_in.at[g, blocks], s_b.at[1, g], r_b.at[1, g], dev(mate, x, y, c))
+
+    def c_copy(zs, h, i):
+        g = zs * 2 + h
+        return remote(c_out.at[g, i], c_in.at[g], s_c.at[i, g], r_c.at[g], dev(far0 + i, x, y, c))
+
+    def stage_a(zs, h):
+        g = zs * 2 + h
+        for x_ in range(X):
+            total = jnp.dot(hid[0], wdn[0, zs * X + x_, h], preferred_element_type=F32)
+            total = total + jnp.dot(hid[1], wdn[1, zs * X + x_, h], preferred_element_type=F32)
+            total = total.reshape(2, Z, q, Dh)
+            a_out[g, :, x_] = total[1].astype(BF16)
+            loc[g, :, x_] = total[0]
+        a_copy(zs, h).start()
+
+    def stage_b(zs, h):
+        g = zs * 2 + h
+        a_copy(zs, h).wait_recv()
+        total = loc[g] + a_in[g].astype(F32)
+        loc[g] = total
+        b_out[g] = total.astype(BF16)
+
+        @pl.when(outer)
+        def _():
+            b_far(zs, h).start()
+
+        b_copy(zs, h).start()
+
+    def stage_c(zs, h):
+        g = zs * 2 + h
+
+        @pl.when(inner)
+        def _():
+            b_far(zs, h).wait_recv()
+            blocks = pl.ds(far0, 2)
+            c_out[g] = (loc[g, blocks] + b_in[g, blocks].astype(F32)).astype(BF16)
+            for i in range(2):
+                c_copy(zs, h, i).start()
+
+        b_copy(zs, h).wait_recv()
+        own_sum = loc[g, z] + b_in[g, z].astype(F32)
+        for x_ in range(X):
+            mid_out[:, cols(zs, x_, h)] = mid_out[:, cols(zs, x_, h)] + own_sum[x_]
+
+    def stage_d(zs, h):
+        g = zs * 2 + h
+        c_copy(zs, h, 0).wait_recv()
+        for x_ in range(X):
+            mid_out[:, cols(zs, x_, h)] = mid_out[:, cols(zs, x_, h)] + c_in[g, x_].astype(F32)
+
+    def fin_copy(to, at):
+        return remote(fin.at[to], fin_in.at[at], s_fin.at[to], r_fin.at[at], (sp, to))
+
+    def stage_e(zs):
+        fin[zs] = mid_out[:, pl.ds(pl.multiple_of(zs * Dl, 128), Dl)].astype(BF16)
+
+        @pl.when(zs != tp)
+        def _():
+            fin_copy(zs, tp).start()
+
+    for h in range(2):
+        own_copy(0, h).wait()
+        hop3(0, h, 0)
+
+    @pl.when(outer)
+    def _():
+        for h in range(2):
+            hop2(0, h, 1)
+            hop3(0, h, 1)
+
+    def mate_hops(hop):
+        @pl.when(inner)
+        def _():
+            for h in range(2):
+                hop(0, h, 1)
+
+    turns = [(half_in, 0), (half_in, 1), (far_in, 0), (half_out, 0), (half_out, 1),
+             (far_in, 1), (far_out, 0), (far_out, 1)]
+    stage_a(*turns[0])
+    hop1(0, 0, 2)
+    stage_a(*turns[1])
+    mate_hops(hop1)
+    stage_b(*turns[0])
+    stage_b(*turns[1])
+    hop2(0, 0, 2)
+    hop1(0, 1, 2)
+    mate_hops(hop2)
+    hop3(0, 0, 2)
+    stage_a(*turns[2])
+    stage_c(*turns[0])
+    stage_c(*turns[1])
+    mate_hops(hop3)
+    stage_a(*turns[3])
+    stage_b(*turns[2])
+    hop1(0, 0, 3)
+    stage_a(*turns[4])
+    stage_b(*turns[3])
+    hop2(0, 1, 2)
+    hop3(0, 1, 2)
+    stage_a(*turns[5])
+    stage_b(*turns[4])
+    stage_c(*turns[2])
+    stage_c(*turns[3])
+    hop2(0, 0, 3)
+    hop1(0, 1, 3)
+    hop3(0, 0, 3)
+    stage_a(*turns[6])
+    stage_b(*turns[5])
+    stage_c(*turns[4])
+    stage_b(*turns[6])
+    stage_c(*turns[5])
+    hop2(0, 1, 3)
+    hop3(0, 1, 3)
+    stage_a(*turns[7])
+    stage_c(*turns[6])
+    stage_b(*turns[7])
+    stage_c(*turns[7])
+    for k, zs in enumerate((half_in, half_out, far_in, far_out)):
+        for h in range(2):
+            stage_d(zs, h)
+        stage_e(zs)
+    out_ref[pl.ds(pl.multiple_of(tp * q, q), q), :] = fin[tp]
+    for k in range(1, ntp):
+        src = lax.rem(tp + k, ntp)
+        fin_copy(src, src).wait_recv()
+        out_ref[pl.ds(pl.multiple_of(src * q, q), q), :] = fin_in[src]
+
+    for up in (1, 0):
+        for h in range(2):
+            for k in range(4):
+                if k > 0:
+                    z_copy(up, h, k).wait_send()
+                x_copy(up, h, k).wait_send()
+                for other in range(2):
+                    d_copy(up, h, k, other).wait_send()
+    for e in range(2):
+        for k in range(1, nsp):
+            ends_do(e, k, True, lambda copy: copy.wait_send())
+    t_far().wait_send()
+    t_mate(0).wait_send()
+
+    @pl.when(inner)
+    def _():
+        for k in (2, 3):
+            t_mate(k).wait_send()
+
+    for k in range(4):
+        y_copy(k).wait_send()
+    for zs in range(Z):
+        for h in range(2):
+            a_copy(zs, h).wait_send()
+            b_copy(zs, h).wait_send()
+
+            @pl.when(outer)
+            def _():
+                b_far(zs, h).wait_send()
+
+            @pl.when(inner)
+            def _():
+                for i in range(2):
+                    c_copy(zs, h, i).wait_send()
+
+        @pl.when(zs != tp)
+        def _():
+            fin_copy(zs, tp).wait_send()
+    for k in range(1, ntp):
+        res_copy(k).wait_send()
+        row_copy(k).wait_send()
+
+
+def paired_call(nsp, ntp, residual, lifted, dts, long_rate, short_rate, emitted, raising):
+    n, W = lifted.shape
+    G = dts.shape[0]
+    half = G // 2
+    PL, PS = long_rate.shape[2], short_rate.shape[2]
+    S = half * (PL + PS)
+    D = emitted.shape[1]
+    Dl = residual.shape[1]
+    q = n // ntp
+    Z, X, Y = mesh_split(nsp, ntp)
+    Fz = raising.shape[1] // Z
+    Dh = D // nsp // 2
+    groups = 2 * Z
+    cfg = (nsp, ntp, n, S, W, G, PL, PS, D, Fz)
+    vm = pl.BlockSpec(memory_space=pltpu.VMEM)
+    dma = pltpu.SemaphoreType.DMA
+    return pl.pallas_call(
+        functools.partial(paired_body, cfg),
+        out_shape=jax.ShapeDtypeStruct((n, Dl), BF16),
+        in_specs=[vm] * 11 + [pl.BlockSpec(memory_space=pl.ANY)] * 5,
+        out_specs=vm,
+        scratch_shapes=[
+            pltpu.VMEM((8, half, CHAN, PL), F32), pltpu.VMEM((8, half, CHAN, PS), F32), dma((2, 8)),
+            pltpu.VMEM((n, S), F32), pltpu.VMEM((n, S), F32),
+            pltpu.VMEM((n, 4 * S), F32), pltpu.VMEM((n, 4 * S), F32),
+            pltpu.VMEM((8, SUB, S), F32), pltpu.VMEM((2, 4, S), F32), pltpu.VMEM((2, nsp - 1, 4, S), F32),
+            pltpu.VMEM((4, SUB, S), F32),
+            pltpu.VMEM((ntp, q, W), BF16), pltpu.VMEM((ntp - 1, q, W), BF16),
+            pltpu.VMEM((q, ntp * W), BF16), pltpu.VMEM(emitted.shape, BF16),
+            pltpu.VMEM((ntp - 1, q, Dl), BF16),
+            pltpu.VMEM((q, D), F32),
+            pltpu.VMEM((2, nsp, 2, D // nsp // 2, Fz), BF16), pltpu.VMEM((2, nsp, 2, Fz, Dh), BF16),
+            pltpu.VMEM((2, Z, q, D), BF16), pltpu.VMEM((2, 2 * Z * q, Fz), BF16),
+            pltpu.VMEM((groups, Z, X, q, Dh), F32),
+            *[pltpu.VMEM((groups, Z, X, q, Dh), BF16)] * 4,
+            pltpu.VMEM((groups, 2, X, q, Dh), BF16), pltpu.VMEM((groups, X, q, Dh), BF16),
+            pltpu.VMEM((ntp, q, Dl), BF16), pltpu.VMEM((ntp, q, Dl), BF16),
+            dma((1,)), dma((2, 2)), *[dma((2, nsp - 1))] * 2, *[dma((ntp - 1,))] * 4,
+            *[dma((2, 2, 4))] * 4, *[dma((2, 2, 4, 2))] * 2, *[dma((4,))] * 4,
+            *[dma((groups,))] * 2, *[dma((2, groups))] * 2, dma((2, groups)), dma((groups,)),
+            *[dma((ntp,))] * 2,
+        ],
+        compiler_params=pltpu.CompilerParams(collective_id=0, has_side_effects=True),
+        cost_estimate=pl.CostEstimate(flops=10**9, bytes_accessed=3 * 10**7, transcendentals=10**6),
+    )
+
+
 def on_device(residual, lifted, dts, fades, long_rate, short_rate, long_freq, short_freq,
               long_lin, short_lin, skip, closing, emitted, leading, raising, lowering):
     nsp, ntp = lax.axis_size("sp"), lax.axis_size("tp")
+    operands = (lifted, dts, fades, long_rate, short_rate, long_freq, short_freq, skip[None], closing[None],
+                residual, leading[None], long_lin.swapaxes(4, 5), short_lin.swapaxes(4, 5), emitted, raising, lowering)
+    Z, X, Y = mesh_split(nsp, ntp)
+    if X == 2 and Y == 2 and Z == ntp:
+        return paired_call(nsp, ntp, residual, lifted, dts, long_rate, short_rate, emitted, raising)(*operands)
     n, W = lifted.shape
     G = dts.shape[0]
     half = G // 2
@@ -471,8 +1132,7 @@
         ],
         compiler_params=pltpu.CompilerParams(collective_id=0, has_side_effects=True),
         cost_estimate=pl.CostEstimate(flops=10**9, bytes_accessed=3 * 10**7, transcendentals=10**6),
-    )(lifted, dts, fades, long_rate, short_rate, long_freq, short_freq, skip[None], closing[None],
-      residual, leading[None], long_lin.swapaxes(4, 5), short_lin.swapaxes(4, 5), emitted, raising, lowering)
+    )(*operands)
 
 
 def solution(mesh):

time: 116 us -> 97 us (0.84)
  the two profiles are of different devices: /device:TPU:31 before, /device:TPU:0 now
where the time goes in v1:
time: 97 us; the launch traced here: 96.9 us
  Pallas kernels  95.3 us (98%)
  local copies, waits for them, and re-layouts  1.57 us (2%)
    pallas_call x1, Pallas kernels, on_device(): paired_call(nsp, ntp, residual, lifted, dts, long_rate, short_rate, emitt...  95.3 us

profile of v1, /device:TPU:0, one launch (start us, length us, event | category | flops | bytes accessed | tf_op | source)
XLA Modules:
  0.0 96.9 jit_solution(5760512924311305536)
XLA Ops:
  0.0 95.3 %shard_map.154 = bf16[128,512]{1,0:T(8,128)(2,1)} custom-call(bf16[128,256]{1,0:T(8,128)(2,1)} %x_ref.1, f32[16,128]{1,0:T(8,128)} %dt_ref.1, f32[16,128]{1,0:T(8,128)} %lf_ref.1, f32[2,32,64]{2,1,0:T(8,128)} %long_rate.1, f32[2,32,32]{2,1,0:T(8,128)} %short_rate.1, f32[2,32,64]{2,1,0:T(8,128)} %long_freq.1, f32[2,32,32]{2,1,0:T(8,128)} %short_freq.1, ...), custom_call_target="tpu_custom_call" | custom-call | flops 1000000000 | bytes 30000000 | tf_op jit(solution)/shard_map/pallas_call | solution.py:1094
  95.3 1.6 %copy.18 = bf16[128,512]{1,0:T(8,128)(2,1)} copy(bf16[128,512]{1,0:T(8,128)(2,1)} %shard_map.154) | data formatting | bytes 262144

commit v2 on v1

--- a/solution.py
+++ b/solution.py
@@ -560,13 +560,16 @@
 
     pl.semaphore_wait(barrier, nsp + ntp - 2)
 
-    @pl.when(inner)
+    @pl.when(outer)
     def _():
         for k in (2, 3):
             z_copy(1, 0, k).start()
 
+    @pl.when(inner)
+    def _():
+        z_copy(1, 0, 1).start()
+
     for h in range(2):
-        z_copy(1, h, 1).start()
         x_copy(1, h, 0).start()
         d_copy(1, h, 0, 0).start()
     for k in range(1, ntp):
@@ -676,30 +679,20 @@
     @pl.when(inner)
     def _():
         for k in (2, 3):
+            z_copy(1, 0, k).start()
+        z_copy(1, 1, 1).start()
+
+    @pl.when(outer)
+    def _():
+        for h in range(2):
+            z_copy(1, h, 1).start()
+        for k in (2, 3):
             z_copy(1, 1, k).start()
-
-    @pl.when(outer)
-    def _():
-        for k in (2, 3):
-            z_copy(1, 0, k).start()
+        hop1(1, 0, 1)
 
     read = jnp.concatenate(
         [block_map(2), block_map(3, -1.0), block_map(6), block_map(7, -1.0)], axis=1)
 
-    for h in range(2):
-        hop1(1, h, 1)
-    for h in range(2):
-        hop2(1, h, 0)
-    hop1(1, 0, 2)
-
-    @pl.when(inner)
-    def _():
-        for h in range(2):
-            z_copy(0, h, 1).start()
-
-    for h in range(2):
-        x_copy(0, h, 0).start()
-        d_copy(0, h, 0, 0).start()
     for k in range(nsp - 1, 0, -1):
         for e in range(2):
             ends_do(e, k, False, lambda copy: copy.wait_recv())
@@ -758,6 +751,22 @@
 
     for k in range(1, ntp):
         row_copy(k).start()
+
+    @pl.when(inner)
+    def _():
+        for h in range(2):
+            z_copy(0, h, 1).start()
+
+    for h in range(2):
+        hop2(1, h, 0)
+
+    hop1(1, 0, 3)
+
+    @pl.when(inner)
+    def _():
+        hop1(1, 0, 1)
+
+    hop1(1, 1, 1)
     emit_copy.wait()
     mrg[:, pl.ds(pl.multiple_of(tp * W, 128), W)] = mg[tp]
     mid_out[:, pl.ds(pl.multiple_of(tp * Dl, 128), Dl)] = resid_ref[pl.ds(pl.multiple_of(tp * q, q), q), :].astype(F32)
@@ -789,58 +798,64 @@
     t_mate(0).start()
     y_copy(0).start()
 
-    @pl.when(outer)
+    @pl.when(inner)
     def _():
         for k in (2, 3):
             z_copy(1, 1, k).start()
+
+    @pl.when(outer)
+    def _():
         for h in range(2):
             z_copy(0, h, 1).start()
 
     for h in range(2):
-        hop2(1, h, 1)
-    hop2(1, 0, 2)
-    hop1(1, 1, 2)
-    hop1(1, 0, 3)
+        x_copy(0, h, 0).start()
+        d_copy(0, h, 0, 0).start()
+
+    hop2(1, 0, 3)
+    hop1(1, 1, 3)
+    hop2(1, 0, 1)
+    hop1(1, 0, 2)
     t_wait(1)
     y_copy(1).start()
 
+    @pl.when(inner)
+    def _():
+        for k in (3, 2):
+            t_wait(k)
+            t_mate(k).start()
+            y_copy(k).start()
+
+    hop2(1, 1, 1)
+    hop2(1, 1, 3)
+    hop2(1, 0, 2)
+
     @pl.when(outer)
     def _():
-        for h in range(2):
-            hop1(0, h, 1)
-
+        t_wait(3)
+        y_copy(3).start()
+        for k in (2, 3):
+            z_copy(0, 0, k).start()
+        t_wait(2)
+        y_copy(2).start()
+
+    hop1(1, 1, 2)
+
+    @pl.when(inner)
+    def _():
+        for k in (2, 3):
+            z_copy(0, 0, k).start()
+
+    @pl.when(outer)
+    def _():
+        for k in (2, 3):
+            z_copy(0, 1, k).start()
+
+    for h in range(2):
+        hop1(0, h, 1)
     for h in range(2):
         hop2(0, h, 0)
     hop2(1, 1, 2)
-    for k in (2, 3):
-        t_wait(k)
-
-        @pl.when(inner)
-        def _():
-            t_mate(k).start()
-
-        y_copy(k).start()
-
-    @pl.when(inner)
-    def _():
-        z_copy(0, 0, 3).start()
-
-    @pl.when(outer)
-    def _():
-        for h in range(2):
-            for k in (2, 3):
-                z_copy(0, h, k).start()
-
-    hop2(1, 0, 3)
-    hop1(1, 1, 3)
-
-    @pl.when(inner)
-    def _():
-        z_copy(0, 0, 2).start()
-        for k in (2, 3):
-            z_copy(0, 1, k).start()
-
-    hop2(1, 1, 3)
     for k in range(4):
         y_copy(k).wait_recv()
     for h in range(2):
@@ -927,64 +942,61 @@
         def _():
             fin_copy(zs, tp).start()
 
+    turns = [(zs, h) for zs in (half_in, half_out, far_out, far_in) for h in range(2)]
+    hop1(0, 0, 3)
+
+    @pl.when(inner)
+    def _():
+        for k in (2, 3):
+            z_copy(0, 1, k).start()
+
     for h in range(2):
         own_copy(0, h).wait()
         hop3(0, h, 0)
-
-    @pl.when(outer)
-    def _():
-        for h in range(2):
-            hop2(0, h, 1)
-            hop3(0, h, 1)
-
-    def mate_hops(hop):
-        @pl.when(inner)
-        def _():
-            for h in range(2):
-                hop(0, h, 1)
-
-    turns = [(half_in, 0), (half_in, 1), (far_in, 0), (half_out, 0), (half_out, 1),
-             (far_in, 1), (far_out, 0), (far_out, 1)]
+    for h in range(2):
+        hop2(0, h, 1)
+    hop1(0, 1, 3)
+    for h in range(2):
+        hop3(0, h, 1)
     stage_a(*turns[0])
+    stage_a(*turns[1])
+    stage_a(*turns[2])
+    stage_a(*turns[3])
+    stage_b(*turns[0])
     hop1(0, 0, 2)
-    stage_a(*turns[1])
-    mate_hops(hop1)
-    stage_b(*turns[0])
+    hop2(0, 0, 3)
     stage_b(*turns[1])
+    hop3(0, 0, 3)
+    stage_a(*turns[4])
+    stage_b(*turns[2])
+    hop2(0, 1, 3)
+    stage_b(*turns[3])
+    hop3(0, 1, 3)
+    stage_a(*turns[5])
+    stage_c(*turns[0])
     hop2(0, 0, 2)
+    stage_c(*turns[1])
     hop1(0, 1, 2)
-    mate_hops(hop2)
     hop3(0, 0, 2)
-    stage_a(*turns[2])
-    stage_c(*turns[0])
-    stage_c(*turns[1])
-    mate_hops(hop3)
-    stage_a(*turns[3])
-    stage_b(*turns[2])
-    hop1(0, 0, 3)
-    stage_a(*turns[4])
-    stage_b(*turns[3])
+    stage_a(*turns[6])
+    stage_c(*turns[2])
+    stage_b(*turns[4])
+    stage_c(*turns[3])
+    stage_b(*turns[5])
     hop2(0, 1, 2)
+    stage_c(*turns[4])
     hop3(0, 1, 2)
-    stage_a(*turns[5])
-    stage_b(*turns[4])
-    stage_c(*turns[2])
-    stage_c(*turns[3])
-    hop2(0, 0, 3)
-    hop1(0, 1, 3)
-    hop3(0, 0, 3)
-    stage_a(*turns[6])
-    stage_b(*turns[5])
-    stage_c(*turns[4])
+    stage_a(*turns[7])
     stage_b(*turns[6])
     stage_c(*turns[5])
-    hop2(0, 1, 3)
-    hop3(0, 1, 3)
-    stage_a(*turns[7])
     stage_c(*turns[6])
     stage_b(*turns[7])
+    for zs in (half_out, far_out):
+        for h in range(2):
+            stage_d(zs, h)
+        stage_e(zs)
     stage_c(*turns[7])
-    for k, zs in enumerate((half_in, half_out, far_in, far_out)):
+    for zs in (far_in, half_in):
         for h in range(2):
             stage_d(zs, h)
         stage_e(zs)

time: 97 us -> 87.5 us (0.902)
  the two profiles are of different devices: /device:TPU:0 before, /device:TPU:1 now
where the time goes in v2:
time: 87.5 us; the launch traced here: 87.3 us
  Pallas kernels  85.7 us (98%)
  local copies, waits for them, and re-layouts  1.57 us (2%)
    pallas_call x1, Pallas kernels, on_device(): paired_call(nsp, ntp, residual, lifted, dts, long_rate, short_rate, emitt...  85.7 us

profile of v2, /device:TPU:1, one launch (start us, length us, event | category | flops | bytes accessed | tf_op | source)
XLA Modules:
  0.0 87.3 jit_solution(4114703319572713376)
XLA Ops:
  0.0 85.7 %shard_map.154 = bf16[128,512]{1,0:T(8,128)(2,1)} custom-call(bf16[128,256]{1,0:T(8,128)(2,1)} %x_ref.1, f32[16,128]{1,0:T(8,128)} %dt_ref.1, f32[16,128]{1,0:T(8,128)} %lf_ref.1, f32[2,32,64]{2,1,0:T(8,128)} %long_rate.1, f32[2,32,32]{2,1,0:T(8,128)} %short_rate.1, f32[2,32,64]{2,1,0:T(8,128)} %long_freq.1, f32[2,32,32]{2,1,0:T(8,128)} %short_freq.1, ...), custom_call_target="tpu_custom_call" | custom-call | flops 1000000000 | bytes 30000000 | tf_op jit(solution)/shard_map/pallas_call | solution.py:1106
  85.7 1.6 %copy.18 = bf16[128,512]{1,0:T(8,128)(2,1)} copy(bf16[128,512]{1,0:T(8,128)(2,1)} %shard_map.154) | data formatting | bytes 262144

commit v3 on v2

--- a/solution.py
+++ b/solution.py
@@ -434,14 +434,15 @@
     return nsp // X, X, Y
 
 
-def paired_body(cfg, x_ref, dt_ref, lf_ref, long_rate, short_rate, long_freq, short_freq,
-                skip_ref, gain_ref, resid_ref, lead_ref, long_hbm, short_hbm, emit_hbm, up_hbm, down_hbm,
-                out_ref, lin_l, lin_s, lin_sem,
+def paired_body(cfg, x_hbm, dt_hbm, lf_hbm, long_rate_hbm, short_rate_hbm, long_freq_hbm, short_freq_hbm,
+                skip_hbm, gain_hbm, resid_hbm, lead_hbm, long_hbm, short_hbm, emit_hbm, up_hbm, down_hbm,
+                out_ref, x_ref, dt_ref, lf_ref, long_rate, short_rate, long_freq, short_freq,
+                skip_ref, gain_ref, resid_ref, lead_ref, in_sem, lin_l, lin_s, lin_sem,
                 pace, surge, pre, st, blk, ends, ends_all, cin, mg, rows_in, mrg, emit, resid_in,
-                mid_out, wup, wdn, nrm, hid, loc, a_out, a_in, b_out, b_in, c_out, c_in, fin, fin_in,
+                mid_out, wup, wdn, nrm, hid, loc, a_out, a_in, b_out, b_in, c_out, c_in, home_in,
                 copy_sem, own_sem, s_ends, r_ends, s_rows, r_rows, s_res, r_res,
-                s_z, r_z, s_x, r_x, s_d, r_d, s_t, r_t, s_y, r_y,
-                s_a, r_a, s_b, r_b, s_c, r_c, s_fin, r_fin):
+                s_z, r_z, s_x, r_x, s_d, r_d_up, r_d_down, s_t, r_t, s_y, r_y,
+                s_a, r_a, s_b, r_b, s_c, r_c, s_last, s_home, r_home):
     nsp, ntp, n, S, W, G, PL, PS, D, Fz = cfg
     Z, X, Y = mesh_split(nsp, ntp)
     L = n // SUB
@@ -473,13 +474,22 @@
         return pltpu.make_async_remote_copy(src_ref=src, dst_ref=dst, send_sem=ssem, recv_sem=rsem,
                                             device_id=to, device_id_type=MESH)
 
+    in_copies = [pltpu.make_async_copy(src, dst, in_sem.at[at]) for at, (src, dst) in enumerate((
+        (dt_hbm, dt_ref), (lf_hbm, lf_ref), (x_hbm, x_ref), (long_rate_hbm, long_rate), (short_rate_hbm, short_rate),
+        (long_freq_hbm, long_freq), (short_freq_hbm, short_freq), (skip_hbm, skip_ref), (gain_hbm, gain_ref),
+        (lead_hbm, lead_ref), (resid_hbm.at[pl.ds(pl.multiple_of(tp * q, q), q), :], resid_ref)))]
     emit_copy = pltpu.make_async_copy(emit_hbm, emit, copy_sem.at[0])
     lin_copies = []
     for at in range(8):
         for kind, (src, dst) in enumerate(((long_hbm, lin_l), (short_hbm, lin_s))):
             lin_copies.append(pltpu.make_async_copy(
-                src.at[at // 4, at // 2 % 2, at % 2, pl.ds(tp * half, half)], dst.at[at],
-                lin_sem.at[kind, at]))
+                src.at[at // 4, at // 2 % 2, at % 2, pl.ds(tp * half, half)], dst.at[at], lin_sem.at[kind]))
+
+    def sent(ref, sem):
+        remote(ref, ref, sem, sem, c_mate).wait_send()
+
+    def came(ref, sem):
+        remote(ref, ref, sem, sem, c_mate).wait_recv()
 
     def bank(up):
         return wup if up else wdn
@@ -491,29 +501,27 @@
         return down_hbm.at[part, pl.ds(h * Dh, Dh)]
 
     def own_copy(up, h):
-        return pltpu.make_async_copy(shard(up, h, z), bank(up).at[c, sp, h], own_sem.at[1 - up, h])
+        return pltpu.make_async_copy(shard(up, h, z), bank(up).at[c, sp, h], own_sem.at[1 - up])
+
+    def own_wait(up):
+        pltpu.make_async_copy(bank(up).at[c, sp], bank(up).at[c, sp], own_sem.at[1 - up]).wait()
 
     def z_copy(up, h, k):
         to = kinds[k]
-        return remote(shard(up, h, to), bank(up).at[c, sp, h], s_z.at[1 - up, h, k],
-                      r_z.at[1 - up, h, 1 if k == 1 else as_seen], dev(to, x, y, c))
-
-    def z_wait(up, h, k):
-        piece = bank(up).at[c, kinds[k] * X + x, h]
-        remote(piece, piece, s_z.at[1 - up, h, k], r_z.at[1 - up, h, k], x_mate).wait_recv()
+        return remote(shard(up, h, to), bank(up).at[c, sp, h], s_z.at[0],
+                      r_z.at[1 - up, h, 0 if k == 1 else as_seen - 1], dev(to, x, y, c))
 
     def x_copy(up, h, k):
         piece = bank(up).at[c, kinds[k] * X + x, h]
-        return remote(shard(up, h, z) if k == 0 else piece, piece,
-                      s_x.at[1 - up, h, k], r_x.at[1 - up, h, k], x_mate)
+        return remote(shard(up, h, z) if k == 0 else piece, piece, s_x.at[0], r_x.at[1 - up, h, k], x_mate)
 
     def d_copy(up, h, k, other):
         piece = bank(up).at[c, kinds[k] * X + (1 - x if other else x), h]
-        return remote(shard(up, h, z) if k == 0 and not other else piece, piece,
-                      s_d.at[1 - up, h, k, other], r_d.at[1 - up, h, k, other], c_mate)
+        return remote(shard(up, h, z) if k == 0 and not other else piece, piece, s_d.at[0],
+                      r_d_up.at[0] if up else r_d_down.at[0 if k < 2 else 1 + (k - 2) * 2 + h], c_mate)
 
     def hop1(up, h, k):
-        z_wait(up, h, k)
+        came(bank(up).at[c, kinds[k] * X + x, h], r_z.at[1 - up, h, k - 1])
         x_copy(up, h, k).start()
         d_copy(up, h, k, 0).start()
 
@@ -521,22 +529,44 @@
         x_copy(up, h, k).wait_recv()
         d_copy(up, h, k, 1).start()
 
-    def hop3(up, h, k):
-        d_copy(up, h, k, 0).wait_recv()
-        d_copy(up, h, k, 1).wait_recv()
+    def hop3_up():
+        came(wup.at[1 - c], r_d_up.at[0])
+
+    def hop3_near():
+        came(wdn.at[1 - c, pl.ds(side * 2 * X, 2 * X)], r_d_down.at[0])
+
+    def hop3_far(h, k):
+        came(wdn.at[1 - c, kinds[k] * X], r_d_down.at[1 + (k - 2) * 2 + h])
 
     def res_copy(k):
         to = lax.rem(tp + k, ntp)
-        return remote(resid_ref.at[pl.ds(to * q, q), :], resid_in.at[k - 1], s_res.at[k - 1], r_res.at[k - 1],
-                      (sp, to))
+        return remote(resid_hbm.at[pl.ds(pl.multiple_of(to * q, q), q), :], resid_in.at[k - 1], s_res.at[0],
+                      r_res.at[0], (sp, to))
 
     barrier = pltpu.get_barrier_semaphore()
     for k in range(1, nsp):
         pl.semaphore_signal(barrier, inc=1, device_id=(lax.rem(sp + k, nsp), tp), device_id_type=MESH)
     for k in range(1, ntp):
         pl.semaphore_signal(barrier, inc=1, device_id=(sp, lax.rem(tp + k, ntp)), device_id_type=MESH)
-    for copy in lin_copies:
+    for copy in in_copies + lin_copies:
         copy.start()
+
+    pl.semaphore_wait(barrier, nsp + ntp - 2)
+
+    @pl.when(outer)
+    def _():
+        for k in (2, 3):
+            z_copy(1, 0, k).start()
+
+    @pl.when(inner)
+    def _():
+        z_copy(1, 0, 1).start()
+
+    for h in range(2):
+        x_copy(1, h, 0).start()
+        d_copy(1, h, 0, 0).start()
+    for k in range(1, ntp):
+        res_copy(k).start()
     emit_copy.start()
     for up in (1, 0):
         for h in range(2):
@@ -555,25 +585,10 @@
         return lax.dot_general(moved, spread, (((0,), (0,)), ((), ())),
                                precision=lax.Precision.HIGHEST, preferred_element_type=F32)
 
+    for copy in in_copies[:2]:
+        copy.wait()
     pace[...] = per_state(dt_ref)
     surge[...] = per_state(lf_ref)
-
-    pl.semaphore_wait(barrier, nsp + ntp - 2)
-
-    @pl.when(outer)
-    def _():
-        for k in (2, 3):
-            z_copy(1, 0, k).start()
-
-    @pl.when(inner)
-    def _():
-        z_copy(1, 0, 1).start()
-
-    for h in range(2):
-        x_copy(1, h, 0).start()
-        d_copy(1, h, 0, 0).start()
-    for k in range(1, ntp):
-        res_copy(k).start()
 
     def flat_kind(ref, e):
         many, states = ref.shape[1:]
@@ -608,9 +623,11 @@
             bands.append(jnp.concatenate([no_long, short_part[band]], axis=1))
         return jnp.concatenate(bands, axis=0)
 
+    for copy in in_copies[2:]:
+        copy.wait()
     xv = jnp.dot(mix.astype(BF16), x_ref[...], preferred_element_type=F32).astype(BF16)
-    for copy in lin_copies:
-        copy.wait()
+    for kind, ref in enumerate((lin_l, lin_s)):
+        pltpu.make_async_copy(ref, ref, lin_sem.at[kind]).wait()
     for e in range(2):
         for part in range(2):
             st[:, pl.ds((2 * e + part) * S, S)] = jnp.dot(
@@ -658,7 +675,7 @@
             ends[e, part : part + 1, :] = run[part]
 
     def ends_copy(e, k):
-        return remote(ends.at[e], ends_all.at[e, k - 1], s_ends.at[e, k - 1], r_ends.at[e, k - 1],
+        return remote(ends.at[e], ends_all.at[e, k - 1], s_ends.at[0], r_ends.at[0],
                       (sp + k if e == 0 else sp - k, tp))
 
     def has_after(e, k):
@@ -667,14 +684,11 @@
     def has_before(e, k):
         return has_after(1 - e, k)
 
-    def ends_do(e, k, send, act):
-        @pl.when(has_after(e, k) if send else has_before(e, k))
-        def _():
-            act(ends_copy(e, k))
-
     for k in range(1, nsp):
         for e in range(2):
-            ends_do(e, k, True, lambda copy: copy.start())
+            @pl.when(has_after(e, k))
+            def _():
+                ends_copy(e, k).start()
 
     @pl.when(inner)
     def _():
@@ -693,9 +707,7 @@
     read = jnp.concatenate(
         [block_map(2), block_map(3, -1.0), block_map(6), block_map(7, -1.0)], axis=1)
 
-    for k in range(nsp - 1, 0, -1):
-        for e in range(2):
-            ends_do(e, k, False, lambda copy: copy.wait_recv())
+    came(ends_all.at[0], r_ends.at[0])
     blank = jnp.zeros((1, S), F32)
 
     def fold(j, carry, e):
@@ -747,7 +759,7 @@
 
     def row_copy(k):
         to = lax.rem(tp + k, ntp)
-        return remote(mg.at[to], rows_in.at[k - 1], s_rows.at[k - 1], r_rows.at[k - 1], (sp, to))
+        return remote(mg.at[to], rows_in.at[k - 1], s_rows.at[0], r_rows.at[0], (sp, to))
 
     for k in range(1, ntp):
         row_copy(k).start()
@@ -769,12 +781,12 @@
     hop1(1, 1, 1)
     emit_copy.wait()
     mrg[:, pl.ds(pl.multiple_of(tp * W, 128), W)] = mg[tp]
-    mid_out[:, pl.ds(pl.multiple_of(tp * Dl, 128), Dl)] = resid_ref[pl.ds(pl.multiple_of(tp * q, q), q), :].astype(F32)
+    mid_out[:, pl.ds(pl.multiple_of(tp * Dl, 128), Dl)] = resid_ref[...].astype(F32)
+    came(resid_in, r_res.at[0])
+    came(rows_in, r_rows.at[0])
     for k in range(1, ntp):
         src = lax.rem(tp - k + ntp, ntp)
-        res_copy(k).wait_recv()
         mid_out[:, pl.ds(pl.multiple_of(src * Dl, 128), Dl)] = resid_in[k - 1].astype(F32)
-        row_copy(k).wait_recv()
         mrg[:, pl.ds(pl.multiple_of(src * W, 128), W)] = rows_in[k - 1]
     mid = mid_out[...] + jnp.dot(mrg[...], emit[...], preferred_element_type=F32)
     mid_out[...] = mid
@@ -782,17 +794,17 @@
     nrm[0, z] = (mid * scale * lead_ref[...]).astype(BF16)
 
     def t_far():
-        return remote(nrm.at[0, z], nrm.at[0, z], s_t.at[0], r_t.at[as_seen], dev(far_in, x, y, c))
+        return remote(nrm.at[0, z], nrm.at[0, z], s_t.at[0], r_t.at[as_seen - 1], dev(far_in, x, y, c))
 
     def t_mate(k):
         block = nrm.at[0, kinds[k]]
-        return remote(block, block, s_t.at[max(k, 1)], r_t.at[max(k, 1)], dev(mate, x, y, c))
+        return remote(block, block, s_t.at[0 if k == 0 else 1], r_t.at[max(k, 1) - 1], dev(mate, x, y, c))
 
     def t_wait(k):
         t_mate(k).wait_recv()
 
     def y_copy(k):
-        return remote(nrm.at[0, kinds[k]], nrm.at[1, kinds[k]], s_y.at[k], r_y.at[k], y_mate)
+        return remote(nrm.at[0, kinds[k]], nrm.at[1, kinds[k]], s_y.at[0], r_y.at[0], y_mate)
 
     t_far().start()
     t_mate(0).start()
@@ -830,24 +842,20 @@
     hop2(1, 1, 3)
     hop2(1, 0, 2)
 
-    @pl.when(outer)
-    def _():
-        t_wait(3)
-        y_copy(3).start()
+    hop1(1, 1, 2)
+
+    @pl.when(inner)
+    def _():
         for k in (2, 3):
             z_copy(0, 0, k).start()
-        t_wait(2)
-        y_copy(2).start()
-
-    hop1(1, 1, 2)
-
-    @pl.when(inner)
-    def _():
-        for k in (2, 3):
-            z_copy(0, 0, k).start()
 
     @pl.when(outer)
     def _():
+        z_copy(0, 0, 2).start()
+        for k in (3, 2):
+            t_wait(k)
+            y_copy(k).start()
+        z_copy(0, 0, 3).start()
         for k in (2, 3):
             z_copy(0, 1, k).start()
 
@@ -856,12 +864,9 @@
     for h in range(2):
         hop2(0, h, 0)
     hop2(1, 1, 2)
-    for k in range(4):
-        y_copy(k).wait_recv()
-    for h in range(2):
-        own_copy(1, h).wait()
-        for k in range(4):
-            hop3(1, h, k)
+    came(nrm.at[1], r_y.at[0])
+    own_wait(1)
+    hop3_up()
     rows = nrm[...].reshape(2 * Z * q, D)
     for b in range(2):
         upward = jnp.dot(rows, wup[b].reshape(D, Fz), preferred_element_type=F32)
@@ -872,20 +877,20 @@
 
     def a_copy(zs, h):
         g = zs * 2 + h
-        return remote(a_out.at[g], a_in.at[g], s_a.at[g], r_a.at[g], y_mate)
+        return remote(a_out.at[g], a_in.at[g], s_a.at[0], r_a.at[g], y_mate)
 
     def b_copy(zs, h):
         g = zs * 2 + h
-        return remote(b_out.at[g, mate], b_in.at[g, mate], s_b.at[0, g], r_b.at[0, g], dev(mate, x, y, c))
+        return remote(b_out.at[g, mate], b_in.at[g, mate], s_b.at[0], r_b.at[0, g], dev(mate, x, y, c))
 
     def b_far(zs, h):
         g = zs * 2 + h
         blocks = pl.ds(far0, 2)
-        return remote(b_out.at[g, blocks], b_in.at[g, blocks], s_b.at[1, g], r_b.at[1, g], dev(mate, x, y, c))
+        return remote(b_out.at[g, blocks], b_in.at[g, blocks], s_b.at[1], r_b.at[1, g], dev(mate, x, y, c))
 
     def c_copy(zs, h, i):
         g = zs * 2 + h
-        return remote(c_out.at[g, i], c_in.at[g], s_c.at[i, g], r_c.at[g], dev(far0 + i, x, y, c))
+        return remote(c_out.at[g, i], c_in.at[tp, h], s_c.at[0], r_c.at[0], ((far0 + i) * X + x, zs))
 
     def stage_a(zs, h):
         g = zs * 2 + h
@@ -926,21 +931,32 @@
         for x_ in range(X):
             mid_out[:, cols(zs, x_, h)] = mid_out[:, cols(zs, x_, h)] + own_sum[x_]
 
-    def stage_d(zs, h):
-        g = zs * 2 + h
-        c_copy(zs, h, 0).wait_recv()
+    def last_copy(zs, to, slot):
+        return remote(b_out.at[zs * 2 + 1, to], c_in.at[tp, slot], s_last.at[0], r_c.at[slot - 1], (to * X + x, zs))
+
+    def last_sums(zs):
+        g = zs * 2 + 1
+        a_copy(zs, 1).wait_recv()
+        loc[g] = loc[g] + a_in[g].astype(F32)
+        b_out[g] = loc[g].astype(BF16)
+        for i in range(2):
+            last_copy(zs, far0 + i, as_seen - 1).start()
+        last_copy(zs, mate, 2).start()
         for x_ in range(X):
-            mid_out[:, cols(zs, x_, h)] = mid_out[:, cols(zs, x_, h)] + c_in[g, x_].astype(F32)
-
-    def fin_copy(to, at):
-        return remote(fin.at[to], fin_in.at[at], s_fin.at[to], r_fin.at[at], (sp, to))
-
-    def stage_e(zs):
-        fin[zs] = mid_out[:, pl.ds(pl.multiple_of(zs * Dl, 128), Dl)].astype(BF16)
+            mid_out[:, cols(zs, x_, 1)] = mid_out[:, cols(zs, x_, 1)] + loc[g, z, x_]
+
+    def home_copy(zs):
+        return remote(mid_out.at[:, pl.ds(pl.multiple_of(zs * Dl, 128), Dl)], home_in.at[tp], s_home.at[0],
+                      r_home.at[0], (sp, zs))
+
+    def stage_d(zs):
+        @pl.when(zs == tp)
+        def _():
+            home_in[tp] = mid_out[:, pl.ds(pl.multiple_of(zs * Dl, 128), Dl)]
 
         @pl.when(zs != tp)
         def _():
-            fin_copy(zs, tp).start()
+            home_copy(zs).start()
 
     turns = [(zs, h) for zs in (half_in, half_out, far_out, far_in) for h in range(2)]
     hop1(0, 0, 3)
@@ -950,103 +966,85 @@
         for k in (2, 3):
             z_copy(0, 1, k).start()
 
-    for h in range(2):
-        own_copy(0, h).wait()
-        hop3(0, h, 0)
+    own_wait(0)
     for h in range(2):
         hop2(0, h, 1)
-    hop1(0, 1, 3)
-    for h in range(2):
-        hop3(0, h, 1)
+    hop3_near()
     stage_a(*turns[0])
     stage_a(*turns[1])
     stage_a(*turns[2])
     stage_a(*turns[3])
+    hop1(0, 1, 3)
     stage_b(*turns[0])
     hop1(0, 0, 2)
     hop2(0, 0, 3)
     stage_b(*turns[1])
-    hop3(0, 0, 3)
+    hop3_far(0, 3)
     stage_a(*turns[4])
     stage_b(*turns[2])
     hop2(0, 1, 3)
     stage_b(*turns[3])
-    hop3(0, 1, 3)
+    hop3_far(1, 3)
     stage_a(*turns[5])
     stage_c(*turns[0])
     hop2(0, 0, 2)
     stage_c(*turns[1])
+    stage_d(half_in)
     hop1(0, 1, 2)
-    hop3(0, 0, 2)
+    hop3_far(0, 2)
     stage_a(*turns[6])
     stage_c(*turns[2])
     stage_b(*turns[4])
     stage_c(*turns[3])
+    stage_d(half_out)
     stage_b(*turns[5])
     hop2(0, 1, 2)
+    stage_b(*turns[6])
+    hop3_far(1, 2)
+    stage_a(*turns[7])
     stage_c(*turns[4])
-    hop3(0, 1, 2)
-    stage_a(*turns[7])
-    stage_b(*turns[6])
     stage_c(*turns[5])
+    stage_d(far_out)
+    last_sums(far_in)
     stage_c(*turns[6])
-    stage_b(*turns[7])
-    for zs in (half_out, far_out):
-        for h in range(2):
-            stage_d(zs, h)
-        stage_e(zs)
-    stage_c(*turns[7])
-    for zs in (far_in, half_in):
-        for h in range(2):
-            stage_d(zs, h)
-        stage_e(zs)
-    out_ref[pl.ds(pl.multiple_of(tp * q, q), q), :] = fin[tp]
-    for k in range(1, ntp):
-        src = lax.rem(tp + k, ntp)
-        fin_copy(src, src).wait_recv()
-        out_ref[pl.ds(pl.multiple_of(src * q, q), q), :] = fin_in[src]
-
-    for up in (1, 0):
-        for h in range(2):
-            for k in range(4):
-                if k > 0:
-                    z_copy(up, h, k).wait_send()
-                x_copy(up, h, k).wait_send()
-                for other in range(2):
-                    d_copy(up, h, k, other).wait_send()
-    for e in range(2):
-        for k in range(1, nsp):
-            ends_do(e, k, True, lambda copy: copy.wait_send())
-    t_far().wait_send()
-    t_mate(0).wait_send()
+    stage_d(far_in)
+    came(home_in.at[pl.ds(0, ntp - 1)], r_home.at[0])
+    came(c_in.at[:, pl.ds(0, 2)], r_c.at[0])
+
+    @pl.when((tp == half_in) | (tp == far_in))
+    def _():
+        came(c_in.at[:, 2], r_c.at[1])
+        for x_ in range(X):
+            at = pl.ds((2 * x_ + 1) * Dh, Dh)
+            home_in[:, :, at] = home_in[:, :, at] + c_in[:, 2, x_].astype(F32)
+
+    for src in range(ntp):
+        for x_ in range(X):
+            for h in range(2):
+                at = pl.ds((2 * x_ + h) * Dh, Dh)
+                out_ref[pl.ds(src * q, q), at] = (home_in[src, :, at] + c_in[src, h, x_].astype(F32)).astype(BF16)
+
+    sent(wup.at[0, pl.ds(0, 6)], s_z.at[0])
+    sent(wup.at[0], s_x.at[0])
+    sent(wup, s_d.at[0])
+    sent(ends_all.at[0], s_ends.at[0])
+    sent(nrm.at[0, pl.ds(0, 2)], s_t.at[0])
+    sent(nrm.at[0], s_y.at[0])
+    sent(a_out, s_a.at[0])
+    sent(b_out.at[pl.ds(0, 2 * Z - 1), 0], s_b.at[0])
+    sent(b_out.at[0, pl.ds(0, 3)], s_last.at[0])
+    sent(home_in.at[pl.ds(0, ntp - 1)], s_home.at[0])
+    sent(resid_in, s_res.at[0])
+    sent(rows_in, s_rows.at[0])
 
     @pl.when(inner)
     def _():
-        for k in (2, 3):
-            t_mate(k).wait_send()
-
-    for k in range(4):
-        y_copy(k).wait_send()
-    for zs in range(Z):
-        for h in range(2):
-            a_copy(zs, h).wait_send()
-            b_copy(zs, h).wait_send()
-
-            @pl.when(outer)
-            def _():
-                b_far(zs, h).wait_send()
-
-            @pl.when(inner)
-            def _():
-                for i in range(2):
-                    c_copy(zs, h, i).wait_send()
-
-        @pl.when(zs != tp)
-        def _():
-            fin_copy(zs, tp).wait_send()
-    for k in range(1, ntp):
-        res_copy(k).wait_send()
-        row_copy(k).wait_send()
+        sent(nrm.at[0, pl.ds(0, 2)], s_t.at[1])
+        sent(c_out.at[pl.ds(0, 2 * Z - 1)], s_c.at[0])
+
+    @pl.when(outer)
+    def _():
+        sent(b_out.at[pl.ds(0, 2 * Z - 1), pl.ds(0, 2)], s_b.at[1])
 
 
 def paired_call(nsp, ntp, residual, lifted, dts, long_rate, short_rate, emitted, raising):
@@ -1068,10 +1066,14 @@
     return pl.pallas_call(
         functools.partial(paired_body, cfg),
         out_shape=jax.ShapeDtypeStruct((n, Dl), BF16),
-        in_specs=[vm] * 11 + [pl.BlockSpec(memory_space=pl.ANY)] * 5,
+        in_specs=[pl.BlockSpec(memory_space=pl.ANY)] * 16,
         out_specs=vm,
         scratch_shapes=[
-            pltpu.VMEM((8, half, CHAN, PL), F32), pltpu.VMEM((8, half, CHAN, PS), F32), dma((2, 8)),
+            pltpu.VMEM(lifted.shape, BF16), pltpu.VMEM(dts.shape, F32), pltpu.VMEM(dts.shape, F32),
+            *[pltpu.VMEM(long_rate.shape, F32), pltpu.VMEM(short_rate.shape, F32)] * 2,
+            pltpu.VMEM((1, ntp * W), F32), pltpu.VMEM((1, ntp * W), F32), pltpu.VMEM((q, Dl), BF16),
+            pltpu.VMEM((1, D), F32), dma((11,)),
+            pltpu.VMEM((8, half, CHAN, PL), F32), pltpu.VMEM((8, half, CHAN, PS), F32), dma((2,)),
             pltpu.VMEM((n, S), F32), pltpu.VMEM((n, S), F32),
             pltpu.VMEM((n, 4 * S), F32), pltpu.VMEM((n, 4 * S), F32),
             pltpu.VMEM((8, SUB, S), F32), pltpu.VMEM((2, 4, S), F32), pltpu.VMEM((2, nsp - 1, 4, S), F32),
@@ -1084,12 +1086,12 @@
             pltpu.VMEM((2, Z, q, D), BF16), pltpu.VMEM((2, 2 * Z * q, Fz), BF16),
             pltpu.VMEM((groups, Z, X, q, Dh), F32),
             *[pltpu.VMEM((groups, Z, X, q, Dh), BF16)] * 4,
-            pltpu.VMEM((groups, 2, X, q, Dh), BF16), pltpu.VMEM((groups, X, q, Dh), BF16),
-            pltpu.VMEM((ntp, q, Dl), BF16), pltpu.VMEM((ntp, q, Dl), BF16),
-            dma((1,)), dma((2, 2)), *[dma((2, nsp - 1))] * 2, *[dma((ntp - 1,))] * 4,
-            *[dma((2, 2, 4))] * 4, *[dma((2, 2, 4, 2))] * 2, *[dma((4,))] * 4,
-            *[dma((groups,))] * 2, *[dma((2, groups))] * 2, dma((2, groups)), dma((groups,)),
-            *[dma((ntp,))] * 2,
+            pltpu.VMEM((groups, 2, X, q, Dh), BF16), pltpu.VMEM((ntp, 3, X, q, Dh), BF16),
+            pltpu.VMEM((ntp, q, Dl), F32),
+            dma((1,)), dma((2,)), *[dma((1,))] * 6,
+            dma((1,)), dma((2, 2, 3)), dma((1,)), dma((2, 2, 4)), dma((1,)), dma((1,)), dma((5,)),
+            dma((2,)), dma((3,)), dma((1,)), dma((1,)),
+            dma((1,)), dma((groups,)), dma((2,)), dma((2, groups)), dma((1,)), dma((2,)), *[dma((1,))] * 3,
         ],
         compiler_params=pltpu.CompilerParams(collective_id=0, has_side_effects=True),
         cost_estimate=pl.CostEstimate(flops=10**9, bytes_accessed=3 * 10**7, transcendentals=10**6),

time: 87.5 us -> 78.8 us (0.901)
  Pallas kernels: 85.7 us -> 77 us
    pallas_call x1, Pallas kernels: 85.7 us -> 77 us  [on_device(): paired_call(nsp, ntp, residual, lifted, dts, long_rate, short_rate, emitt...]
where the time goes in v3:
time: 78.8 us; the launch traced here: 78.6 us
  Pallas kernels  77 us (98%)
  local copies, waits for them, and re-layouts  1.57 us (2%)
    pallas_call x1, Pallas kernels, on_device(): paired_call(nsp, ntp, residual, lifted, dts, long_rate, short_rate, emitt...  77 us

profile of v3, /device:TPU:1, one launch (start us, length us, event | category | flops | bytes accessed | tf_op | source)
XLA Modules:
  0.0 78.6 jit_solution(6678936129668613727)
XLA Ops:
  0.0 77.0 %shard_map.154 = bf16[128,512]{1,0:T(8,128)(2,1)} custom-call(bf16[128,256]{1,0:T(8,128)(2,1)} %x_hbm.1, f32[16,128]{1,0:T(8,128)} %dt_hbm.1, f32[16,128]{1,0:T(8,128)} %lf_hbm.1, f32[2,32,64]{2,1,0:T(8,128)} %long_rate_hbm.1, f32[2,32,32]{2,1,0:T(8,128)} %short_rate_hbm.1, f32[2,32,64]{2,1,0:T(8,128)} %long_freq_hbm.1, f32[2,32,32]{2,1,0:T(8,128)} %short_freq_hbm.1, ...), custom_call_target="tpu_custom_call" | custom-call | flops 1000000000 | bytes 30000000 | tf_op jit(solution)/shard_map/pallas_call | solution.py:1108
  77.0 1.6 %copy.18 = bf16[128,512]{1,0:T(8,128)(2,1)} copy(bf16[128,512]{1,0:T(8,128)(2,1)} %shard_map.154) | data formatting | bytes 262144

commit v4 on v3

--- a/solution.py
+++ b/solution.py
@@ -11,6 +11,7 @@
 NORM_W = 128
 EPSILON = 1e-06
 SUB = 8
+PARTS = 4
 F32, BF16 = jnp.float32, jnp.bfloat16
 
 
@@ -442,7 +443,8 @@
                 mid_out, wup, wdn, nrm, hid, loc, a_out, a_in, b_out, b_in, c_out, c_in, home_in,
                 copy_sem, own_sem, s_ends, r_ends, s_rows, r_rows, s_res, r_res,
                 s_z, r_z, s_x, r_x, s_d, r_d_up, r_d_down, s_t, r_t, s_y, r_y,
-                s_a, r_a, s_b, r_b, s_c, r_c, s_last, s_home, r_home):
+                s_a, r_a, s_b, r_b, s_c, r_c, s_last, s_home, r_home,
+                o_out, s_own, r_own, r_tz, r_tx, r_td, r_ta):
     nsp, ntp, n, S, W, G, PL, PS, D, Fz = cfg
     Z, X, Y = mesh_split(nsp, ntp)
     L = n // SUB
@@ -525,6 +527,34 @@
         x_copy(up, h, k).start()
         d_copy(up, h, k, 0).start()
 
+    def tail_rows(part):
+        return pl.ds(part * (Fz // PARTS), Fz // PARTS)
+
+    def tail_send(part, k):
+        to = kinds[k]
+        src = down_hbm.at[pl.ds(pl.multiple_of(to * Fz + part * (Fz // PARTS), 16), Fz // PARTS), pl.ds(Dh, Dh)]
+        return remote(src, wdn.at[c, sp, 1, tail_rows(part)], s_z.at[0], r_tz.at[part], dev(to, x, y, c))
+
+    def tail_x(part):
+        piece = wdn.at[c, far_in * X + x, 1, tail_rows(part)]
+        return remote(piece, piece, s_x.at[0], r_tx.at[part], x_mate)
+
+    def tail_d(part, other):
+        piece = wdn.at[c, far_in * X + (1 - x if other else x), 1, tail_rows(part)]
+        return remote(piece, piece, s_d.at[0], r_td.at[other], c_mate)
+
+    def tail1(part):
+        came(wdn.at[c, far_in * X + x, 1, tail_rows(part)], r_tz.at[part])
+        tail_x(part).start()
+        tail_d(part, 0).start()
+
+    def tail2(part):
+        tail_x(part).wait_recv()
+        tail_d(part, 1).start()
+
+    def tail3(other):
+        came(wdn.at[1 - c, far_in * X + (1 - x if other else x), 1], r_td.at[other])
+
     def hop2(up, h, k):
         x_copy(up, h, k).wait_recv()
         d_copy(up, h, k, 1).start()
@@ -915,6 +945,15 @@
 
         b_copy(zs, h).start()
 
+    def keep(zs, src, dst):
+        @pl.when(zs == tp)
+        def _():
+            dst[...] = src[...]
+
+        @pl.when(zs != tp)
+        def _():
+            remote(src, dst, s_own.at[0], r_own.at[0], (sp, zs)).start()
+
     def stage_c(zs, h):
         g = zs * 2 + h
 
@@ -927,44 +966,55 @@
                 c_copy(zs, h, i).start()
 
         b_copy(zs, h).wait_recv()
-        own_sum = loc[g, z] + b_in[g, z].astype(F32)
-        for x_ in range(X):
-            mid_out[:, cols(zs, x_, h)] = mid_out[:, cols(zs, x_, h)] + own_sum[x_]
-
-    def last_copy(zs, to, slot):
-        return remote(b_out.at[zs * 2 + 1, to], c_in.at[tp, slot], s_last.at[0], r_c.at[slot - 1], (to * X + x, zs))
-
-    def last_sums(zs):
-        g = zs * 2 + 1
-        a_copy(zs, 1).wait_recv()
-        loc[g] = loc[g] + a_in[g].astype(F32)
-        b_out[g] = loc[g].astype(BF16)
+        o_out[g] = (loc[g, z] + b_in[g, z].astype(F32)).astype(BF16)
+        keep(zs, o_out.at[g], c_in.at[tp, 3 + h])
+
+    last = far_in * 2 + 1
+
+    def tail_copy(xd, other):
+        return remote(a_out.at[last, :, xd], a_in.at[last, :, xd], s_a.at[0], r_ta.at[other], y_mate)
+
+    def tail_a(other):
+        xd = 1 - x if other else x
+        total = jnp.dot(hid[0], wdn[0, far_in * X + xd, 1], preferred_element_type=F32)
+        total = total + jnp.dot(hid[1], wdn[1, far_in * X + xd, 1], preferred_element_type=F32)
+        total = total.reshape(2, Z, q, Dh)
+        a_out[last, :, xd] = total[1].astype(BF16)
+        loc[last, :, xd] = total[0]
+        tail_copy(xd, other).start()
+
+    def tail_sums(other):
+        xd = 1 - x if other else x
+        tail_copy(xd, other).wait_recv()
+        b_out[last, :, xd] = (loc[last, :, xd] + a_in[last, :, xd].astype(F32)).astype(BF16)
         for i in range(2):
-            last_copy(zs, far0 + i, as_seen - 1).start()
-        last_copy(zs, mate, 2).start()
-        for x_ in range(X):
-            mid_out[:, cols(zs, x_, 1)] = mid_out[:, cols(zs, x_, 1)] + loc[g, z, x_]
+            to = far0 + i
+            remote(b_out.at[last, to, xd], c_in.at[tp, as_seen - 1, xd], s_last.at[0], r_c.at[as_seen - 2],
+                   (to * X + x, far_in)).start()
+        remote(b_out.at[last, mate, xd], c_in.at[tp, 2, xd], s_last.at[0], r_c.at[1], (mate * X + x, far_in)).start()
+        keep(far_in, b_out.at[last, z, xd], c_in.at[tp, 4, xd])
 
     def home_copy(zs):
         return remote(mid_out.at[:, pl.ds(pl.multiple_of(zs * Dl, 128), Dl)], home_in.at[tp], s_home.at[0],
                       r_home.at[0], (sp, zs))
 
-    def stage_d(zs):
+    turns = [(zs, h) for zs in (half_in, half_out, far_out, far_in) for h in range(2)]
+    hop1(0, 0, 3)
+
+    @pl.when(inner)
+    def _():
+        for part in range(PARTS):
+            for k in (2, 3):
+                tail_send(part, k).start()
+
+    for zs in range(Z):
         @pl.when(zs == tp)
         def _():
-            home_in[tp] = mid_out[:, pl.ds(pl.multiple_of(zs * Dl, 128), Dl)]
+            home_in[tp] = mid_out[:, zs * Dl : (zs + 1) * Dl]
 
         @pl.when(zs != tp)
         def _():
             home_copy(zs).start()
-
-    turns = [(zs, h) for zs in (half_in, half_out, far_out, far_in) for h in range(2)]
-    hop1(0, 0, 3)
-
-    @pl.when(inner)
-    def _():
-        for k in (2, 3):
-            z_copy(0, 1, k).start()
 
     own_wait(0)
     for h in range(2):
@@ -976,39 +1026,45 @@
     stage_a(*turns[3])
     hop1(0, 1, 3)
     stage_b(*turns[0])
-    hop1(0, 0, 2)
     hop2(0, 0, 3)
     stage_b(*turns[1])
+    hop1(0, 0, 2)
     hop3_far(0, 3)
     stage_a(*turns[4])
     stage_b(*turns[2])
     hop2(0, 1, 3)
+    tail1(0)
     stage_b(*turns[3])
+    tail1(1)
     hop3_far(1, 3)
     stage_a(*turns[5])
+    stage_b(*turns[4])
+    hop2(0, 0, 2)
+    tail1(2)
     stage_c(*turns[0])
-    hop2(0, 0, 2)
-    stage_c(*turns[1])
-    stage_d(half_in)
-    hop1(0, 1, 2)
+    tail1(3)
     hop3_far(0, 2)
     stage_a(*turns[6])
+    tail2(0)
+    stage_c(*turns[1])
     stage_c(*turns[2])
-    stage_b(*turns[4])
+    tail2(1)
+    tail3(0)
+    tail_a(0)
     stage_c(*turns[3])
-    stage_d(half_out)
+    tail2(2)
     stage_b(*turns[5])
-    hop2(0, 1, 2)
+    tail2(3)
+    tail3(1)
+    tail_a(1)
     stage_b(*turns[6])
-    hop3_far(1, 2)
-    stage_a(*turns[7])
+    tail_sums(0)
     stage_c(*turns[4])
     stage_c(*turns[5])
-    stage_d(far_out)
-    last_sums(far_in)
+    tail_sums(1)
     stage_c(*turns[6])
-    stage_d(far_in)
     came(home_in.at[pl.ds(0, ntp - 1)], r_home.at[0])
+    came(c_in.at[pl.ds(0, ntp - 1), pl.ds(3, 2)], r_own.at[0])
     came(c_in.at[:, pl.ds(0, 2)], r_c.at[0])
 
     @pl.when((tp == half_in) | (tp == far_in))
@@ -1022,7 +1078,8 @@
         for x_ in range(X):
             for h in range(2):
                 at = pl.ds((2 * x_ + h) * Dh, Dh)
-                out_ref[pl.ds(src * q, q), at] = (home_in[src, :, at] + c_in[src, h, x_].astype(F32)).astype(BF16)
+                total = home_in[src, :, at] + c_in[src, h, x_].astype(F32) + c_in[src, 3 + h, x_].astype(F32)
+                out_ref[pl.ds(src * q, q), at] = total.astype(BF16)
 
     sent(wup.at[0, pl.ds(0, 6)], s_z.at[0])
     sent(wup.at[0], s_x.at[0])
@@ -1033,6 +1090,7 @@
     sent(a_out, s_a.at[0])
     sent(b_out.at[pl.ds(0, 2 * Z - 1), 0], s_b.at[0])
     sent(b_out.at[0, pl.ds(0, 3)], s_last.at[0])
+    sent(c_in.at[pl.ds(0, ntp - 1), pl.ds(3, 2)], s_own.at[0])
     sent(home_in.at[pl.ds(0, ntp - 1)], s_home.at[0])
     sent(resid_in, s_res.at[0])
     sent(rows_in, s_rows.at[0])
@@ -1086,12 +1144,13 @@
             pltpu.VMEM((2, Z, q, D), BF16), pltpu.VMEM((2, 2 * Z * q, Fz), BF16),
             pltpu.VMEM((groups, Z, X, q, Dh), F32),
             *[pltpu.VMEM((groups, Z, X, q, Dh), BF16)] * 4,
-            pltpu.VMEM((groups, 2, X, q, Dh), BF16), pltpu.VMEM((ntp, 3, X, q, Dh), BF16),
+            pltpu.VMEM((groups, 2, X, q, Dh), BF16), pltpu.VMEM((ntp, 5, X, q, Dh), BF16),
             pltpu.VMEM((ntp, q, Dl), F32),
             dma((1,)), dma((2,)), *[dma((1,))] * 6,
             dma((1,)), dma((2, 2, 3)), dma((1,)), dma((2, 2, 4)), dma((1,)), dma((1,)), dma((5,)),
             dma((2,)), dma((3,)), dma((1,)), dma((1,)),
             dma((1,)), dma((groups,)), dma((2,)), dma((2, groups)), dma((1,)), dma((2,)), *[dma((1,))] * 3,
+            pltpu.VMEM((groups, X, q, Dh), BF16), dma((1,)), dma((1,)), dma((PARTS,)), dma((PARTS,)), dma((2,)), dma((2,)),
         ],
         compiler_params=pltpu.CompilerParams(collective_id=0, has_side_effects=True),
         cost_estimate=pl.CostEstimate(flops=10**9, bytes_accessed=3 * 10**7, transcendentals=10**6),

time: 78.8 us -> 76.7 us (0.973)
  Pallas kernels: 77 us -> 75 us
    pallas_call x1, Pallas kernels: 77 us -> 75 us  [on_device(): paired_call(nsp, ntp, residual, lifted, dts, long_rate, short_rate, emitt...]
where the time goes in v4:
time: 76.7 us; the launch traced here: 76.6 us
  Pallas kernels  75 us (98%)
  local copies, waits for them, and re-layouts  1.57 us (2%)
    pallas_call x1, Pallas kernels, on_device(): paired_call(nsp, ntp, residual, lifted, dts, long_rate, short_rate, emitt...  75 us
    unnamed x1, local copies, waits for them, and re-layouts  1.57 us

profile of v4, /device:TPU:1, one launch (start us, length us, event | category | flops | bytes accessed | tf_op | source)
XLA Modules:
  0.0 76.6 jit_solution(5614131825927892254)
XLA Ops:
  0.0 75.0 %shard_map.154 = bf16[128,512]{1,0:T(8,128)(2,1)} custom-call(bf16[128,256]{1,0:T(8,128)(2,1)} %x_hbm.1, f32[16,128]{1,0:T(8,128)} %dt_hbm.1, f32[16,128]{1,0:T(8,128)} %lf_hbm.1, f32[2,32,64]{2,1,0:T(8,128)} %long_rate_hbm.1, f32[2,32,32]{2,1,0:T(8,128)} %short_rate_hbm.1, f32[2,32,64]{2,1,0:T(8,128)} %long_freq_hbm.1, f32[2,32,32]{2,1,0:T(8,128)} %short_freq_hbm.1, ...), custom_call_target="tpu_custom_call" | custom-call | flops 1000000000 | bytes 30000000 | tf_op jit(solution)/shard_map/pallas_call | solution.py:1167
  75.0 1.6 %copy.18 = bf16[128,512]{1,0:T(8,128)(2,1)} copy(bf16[128,512]{1,0:T(8,128)(2,1)} %shard_map.154) | data formatting | bytes 262144

commit v5 on v4

--- a/solution.py
+++ b/solution.py
@@ -435,6 +435,14 @@
     return nsp // X, X, Y
 
 
+def thirds(a):
+    high = a.astype(BF16)
+    rest = a - high.astype(F32)
+    middle = rest.astype(BF16)
+    low = (rest - middle.astype(F32)).astype(BF16)
+    return jnp.concatenate([high, middle, low], axis=0)
+
+
 def paired_body(cfg, x_hbm, dt_hbm, lf_hbm, long_rate_hbm, short_rate_hbm, long_freq_hbm, short_freq_hbm,
                 skip_hbm, gain_hbm, resid_hbm, lead_hbm, long_hbm, short_hbm, emit_hbm, up_hbm, down_hbm,
                 out_ref, x_ref, dt_ref, lf_ref, long_rate, short_rate, long_freq, short_freq,
@@ -604,30 +612,29 @@
 
     lane = lax.broadcasted_iota(jnp.int32, (G, S), 1)
     group = jnp.where(lane < SL, 2 * (lane // PL), 2 * ((lane - SL) // PS) + 1)
-    spread = (group == lax.broadcasted_iota(jnp.int32, (G, S), 0)).astype(F32)
+    spread = (group == lax.broadcasted_iota(jnp.int32, (G, S), 0)).astype(BF16)
     r = lax.broadcasted_iota(jnp.int32, (n, n), 0)
     t = lax.broadcasted_iota(jnp.int32, (n, n), 1)
-    mix = (t == (r % SUB) * L + r // SUB).astype(F32)
-
-    def per_state(ref):
-        moved = lax.dot_general(ref[...], mix, (((1,), (1,)), ((), ())),
-                                precision=lax.Precision.HIGHEST, preferred_element_type=F32)
-        return lax.dot_general(moved, spread, (((0,), (0,)), ((), ())),
-                               precision=lax.Precision.HIGHEST, preferred_element_type=F32)
+    mix = (t == (r % SUB) * L + r // SUB).astype(BF16)
+
+    spread = jnp.concatenate([spread] * 3, axis=0)
 
     for copy in in_copies[:2]:
         copy.wait()
-    pace[...] = per_state(dt_ref)
-    surge[...] = per_state(lf_ref)
-
+    moved = lax.dot_general(jnp.concatenate([thirds(dt_ref[...]), thirds(lf_ref[...])], axis=0), mix,
+                            (((1,), (1,)), ((), ())), preferred_element_type=F32).astype(BF16)
+    pace[...], surge[...] = (
+        lax.dot_general(moved[3 * G * at : 3 * G * (at + 1)], spread, (((0,), (0,)), ((), ())),
+                        preferred_element_type=F32) for at in range(2))
     def flat_kind(ref, e):
-        many, states = ref.shape[1:]
+        states = ref.shape[2]
         width = half * states
         repeat = (lax.broadcasted_iota(jnp.int32, (states, width), 1) % states
-                  == lax.broadcasted_iota(jnp.int32, (states, width), 0)).astype(F32)
-        wide = jnp.dot(ref[e], repeat, precision=lax.Precision.HIGHEST, preferred_element_type=F32)
-        owner = tp * half + lax.broadcasted_iota(jnp.int32, (many, width), 1) // states
-        mine = owner == lax.broadcasted_iota(jnp.int32, (many, width), 0)
+                  == lax.broadcasted_iota(jnp.int32, (states, width), 0)).astype(BF16)
+        own_rows = ref[e, pl.ds(pl.multiple_of(tp * half, half), half), :]
+        wide = jnp.dot(thirds(own_rows), repeat, preferred_element_type=F32)
+        mine = (lax.broadcasted_iota(jnp.int32, (3 * half, width), 0) % half
+                == lax.broadcasted_iota(jnp.int32, (3 * half, width), 1) // states)
         return jnp.sum(jnp.where(mine, wide, 0.0), axis=0, keepdims=True)
 
     def flat(long_ref, short_ref, e):
@@ -655,7 +662,7 @@
 
     for copy in in_copies[2:]:
         copy.wait()
-    xv = jnp.dot(mix.astype(BF16), x_ref[...], preferred_element_type=F32).astype(BF16)
+    xv = jnp.dot(mix, x_ref[...], preferred_element_type=F32).astype(BF16)
     for kind, ref in enumerate((lin_l, lin_s)):
         pltpu.make_async_copy(ref, ref, lin_sem.at[kind]).wait()
     for e in range(2):

time: 76.7 us -> 76.7 us (level)
  no operation moved by 1% of the time
where the time goes in v5:
time: 76.7 us; the launch traced here: 76.5 us
  Pallas kernels  74.9 us (98%)
  local copies, waits for them, and re-layouts  1.57 us (2%)
    pallas_call x1, Pallas kernels, on_device(): paired_call(nsp, ntp, residual, lifted, dts, long_rate, short_rate, emitt...  74.9 us
    unnamed x1, local copies, waits for them, and re-layouts  1.57 us

profile of v5, /device:TPU:1, one launch (start us, length us, event | category | flops | bytes accessed | tf_op | source)
XLA Modules:
  0.0 76.5 jit_solution(17439812972599733675)
XLA Ops:
  0.0 74.9 %shard_map.154 = bf16[128,512]{1,0:T(8,128)(2,1)} custom-call(bf16[128,256]{1,0:T(8,128)(2,1)} %x_hbm.1, f32[16,128]{1,0:T(8,128)} %dt_hbm.1, f32[16,128]{1,0:T(8,128)} %lf_hbm.1, f32[2,32,64]{2,1,0:T(8,128)} %long_rate_hbm.1, f32[2,32,32]{2,1,0:T(8,128)} %short_rate_hbm.1, f32[2,32,64]{2,1,0:T(8,128)} %long_freq_hbm.1, f32[2,32,32]{2,1,0:T(8,128)} %short_freq_hbm.1, ...), custom_call_target="tpu_custom_call" | custom-call | flops 1000000000 | bytes 30000000 | tf_op jit(solution)/shard_map/pallas_call | solution.py:1174
  74.9 1.6 %copy.18 = bf16[128,512]{1,0:T(8,128)(2,1)} copy(bf16[128,512]{1,0:T(8,128)(2,1)} %shard_map.154) | data formatting | bytes 262144
